TPU v7x, 32 devices: a whole 2x2x4 slice. The times are simulated.
32 devices in a mesh: dp: 4 (over y, x), kv: 4 (over z), tp: 2 (over core).
Axes of the slice: x: 2, y: 2, z: 4, core: 2. Of those that a mesh axis runs over, the one named last changes fastest.
Arguments:
- pieces: bfloat16 [4096, 8, 2048], P(('kv', 'tp'), 'dp'), parts along dimension 1, may hold values from -6 to 6
- new_tokens: bfloat16 [256, 2048], P(('dp', 'kv', 'tp')), parts along dimension 0, may hold values from -6 to 6
- w_query: bfloat16 [2048, 1024], P(None, 'tp'), may hold values from -0.125 to 0.125
- w_key: bfloat16 [2048, 1024], P(None, 'tp'), may hold values from -0.125 to 0.125
- w_value: bfloat16 [2048, 2048], P(None, 'tp'), may hold values from -0.125 to 0.125
- w_decay: bfloat16 [2048, 1024], P(None, 'tp'), may hold values from -0.125 to 0.125
- decay_bias: float32 [1024], replicated, may hold values from 0 to 9
- norm_gain: float32 [2048], replicated, may hold values from 0.1 to 1.9
- head_gain: float32 [2048], replicated, may hold values from 0.1 to 1.9
- w_out: bfloat16 [2048, 2048], replicated, may hold values from -0.125 to 0.125
- prompt_state: float32 [8, 8, 128, 256], P('dp', 'tp', 'kv'), parts along dimension 0, may hold values from -8 to 8
- decode_state: float32 [256, 8, 128, 256], P(('dp', 'kv'), 'tp'), parts along dimension 0, may hold values from -8 to 8
Outputs:
- mixed_piece: bfloat16 [4096, 8, 2048], P(('kv', 'tp'), 'dp'), parts along dimension 1
- mixed_decode: bfloat16 [256, 2048], P(('dp', 'kv', 'tp')), parts along dimension 0
- prompt_state_out: float32 [8, 8, 128, 256], P('dp', 'tp', 'kv'), parts along dimension 0
- decode_state_out: float32 [256, 8, 128, 256], P(('dp', 'kv'), 'tp'), parts along dimension 0
There are 4 independent parts, one for each index of `dp`. A program takes and returns all parts, laid end to end along the dimension named above; an argument that names none is the same for every part. Nothing has to cross between parts.
All inputs are finite; a program needn't handle non-finite values.
Results may differ from a plain program's by a relative error of at most 0.014.
Values may be sent and summed in bfloat16 or wider, within the bound.
A program may use at most 192 MiB of HBM per device.

v0:
```python
import functools

import jax
import jax.numpy as jnp
import numpy as np
from jax import lax
from jax.experimental import pallas as pl
from jax.experimental.pallas import tpu as pltpu
from jax.sharding import PartitionSpec as P

DK = 128
DV = 256
STEP = 64
PART = 16

norm_eps = 0.1
decay_tau = 16.0
f32, bf16 = jnp.float32, jnp.bfloat16
MESH = pl.DeviceIdType.MESH
PAD = 16


def dot(a, b):
    return jnp.dot(a, b, preferred_element_type=f32)


def dot_nt(a, b):
    return lax.dot_general(a, b, (((1,), (1,)), ((), ())), preferred_element_type=f32)


def dot_tn(a, b):
    return lax.dot_general(a, b, (((0,), (0,)), ((), ())), preferred_element_type=f32)


def sum_matrices(prompts):
    n = STEP * prompts
    r, c = np.arange(n)[:, None], np.arange(n)[None]
    same = (r % prompts) == (c % prompts)

    def from_anchor(edge):
        return (same & (c >= edge) & (c <= r)) * 1.0 - (same & (c < edge) & (c > r)) * 1.0

    b = (same & (c <= r)) * 1.0
    rest = (same & (c > r)) * 1.0
    d0 = from_anchor(PART * prompts)[: n // 2]
    d1 = from_anchor(3 * PART * prompts)
    one = np.concatenate([b, rest, d0, d1], axis=0)
    return np.concatenate([one, one, one], axis=1)


def meet_partner(other):
    barrier = pltpu.get_barrier_semaphore()
    pl.semaphore_signal(barrier, inc=1, device_id={"tp": other}, device_id_type=MESH)
    pl.semaphore_wait(barrier, 1)


def front_kernel(
    own, chunk, prompts, heads,
    x_hbm, dec_ref, wq_hbm, wk_hbm, wv_hbm, wd_hbm, bias_ref, gain_ref, mats_ref,
    out_ref, qt_ref, st_ref, tot_ref, dp_ref,
    xb, nb, nd, wq, wk, wv, wd, qs, ks, vs, gs,
    x_sem, w_sem, send_sem, recv_sem, dsend, drecv,
):
    me = lax.axis_index("tp")
    other = 1 - me
    count = own // chunk
    for j in range(count):
        pltpu.make_async_copy(x_hbm.at[pl.ds(j * chunk, chunk)], xb.at[pl.ds(j * chunk, chunk)], x_sem.at[j]).start()
    loads = [
        pltpu.make_async_copy(src, dst, w_sem.at[i])
        for i, (src, dst) in enumerate(((wq_hbm, wq), (wk_hbm, wk), (wv_hbm, wv), (wd_hbm, wd)))
    ]
    for load in loads:
        load.start()
    meet_partner(other)

    def normed(rows):
        wide = rows.astype(f32)
        factor = lax.rsqrt(jnp.mean(wide * wide, axis=-1, keepdims=True) + norm_eps)
        return (wide * factor * gain_ref[...]).astype(bf16)

    def piece_copy(j):
        rows = pl.ds(pl.multiple_of(me * own + j * chunk, chunk), chunk)
        return pltpu.make_async_remote_copy(
            src_ref=nb.at[rows], dst_ref=nb.at[rows], send_sem=send_sem.at[j], recv_sem=recv_sem.at[j],
            device_id={"tp": other}, device_id_type=MESH,
        )

    mine = pl.ds(pl.multiple_of(me * PAD, PAD), PAD)
    nd[mine, :] = normed(dec_ref[...])
    dec_copy = pltpu.make_async_remote_copy(
        src_ref=nd.at[mine], dst_ref=nd.at[mine], send_sem=dsend, recv_sem=drecv,
        device_id={"tp": other}, device_id_type=MESH,
    )
    small = min(64, chunk)
    for j in range(count):
        pltpu.make_async_copy(x_hbm.at[pl.ds(j * chunk, chunk)], xb.at[pl.ds(j * chunk, chunk)], x_sem.at[j]).wait()

        @pl.loop(0, chunk // small)
        def _(s):
            at = j * chunk + s * small
            nb[pl.ds(pl.multiple_of(me * own + at, small), small), :] = normed(xb[pl.ds(pl.multiple_of(at, small), small), :])

        if j == 0:
            dec_copy.start()
        else:
            piece_copy(j - 1).start()
    piece_copy(count - 1).start()
    for load in loads:
        load.wait()

    def decay_of(product):
        t = product + bias_ref[...]
        return (jnp.minimum(t, 0.0) - jnp.log1p(jnp.exp(-jnp.abs(t)))) * (1.0 / decay_tau)

    def project(at):
        rows = pl.ds(pl.multiple_of(at, chunk), chunk)
        block = nb[rows, :]
        qs[rows, :] = (dot(block, wq[...]) * DK ** (-0.5)).astype(bf16)
        ks[rows, :] = dot(block, wk[...]).astype(bf16)
        half = wv.shape[1] // 2
        vs[rows, :half] = dot(block, wv[:, :half]).astype(bf16)
        vs[rows, half:] = dot(block, wv[:, half:]).astype(bf16)
        gs[rows, :] = decay_of(dot(block, wd[...]))

    @pl.loop(0, count)
    def _(j):
        project(me * own + j * chunk)

    @pl.loop(0, count)
    def _(j):
        rows = pl.ds(pl.multiple_of(other * own + j * chunk, chunk), chunk)
        pltpu.make_async_remote_copy(
            src_ref=nb.at[rows], dst_ref=nb.at[rows], send_sem=send_sem.at[j], recv_sem=recv_sem.at[j],
            device_id={"tp": other}, device_id_type=MESH,
        ).wait_recv()
        project(other * own + j * chunk)

    for j in range(count):
        piece_copy(j).wait_send()
    dec_copy.wait()
    dec_rows = nd[...]
    qk = wq.shape[1]
    dp_ref[:, :qk] = (dot(dec_rows, wq[...]) * DK ** (-0.5)).astype(bf16).astype(f32)
    dp_ref[:, qk : 2 * qk] = dot(dec_rows, wk[...]).astype(bf16).astype(f32)
    dp_ref[:, 2 * qk : 3 * qk] = decay_of(dot(dec_rows, wd[...]))
    dp_ref[:, 3 * qk :] = dot(dec_rows, wv[...]).astype(bf16).astype(f32)

    n = STEP * prompts
    half = n // 2
    st_ref[...] = jnp.zeros_like(st_ref)
    tot_ref[...] = jnp.zeros_like(tot_ref)

    @pl.loop(0, 2 * own // n)
    def _(i):
        rows = pl.ds(pl.multiple_of(i * n, n), n)
        g = gs[rows, :]
        hi = g.astype(bf16)
        left = g - hi.astype(f32)
        mid = left.astype(bf16)
        low = (left - mid.astype(f32)).astype(bf16)
        sums = dot(mats_ref[...], jnp.concatenate([hi, mid, low], axis=0))
        b, rest = sums[:n], sums[n : 2 * n]
        d0, d1 = sums[2 * n : 2 * n + half], sums[2 * n + half :]
        q = qs[rows, :].astype(f32)
        k = ks[rows, :].astype(f32)
        row_prompt = lax.broadcasted_iota(jnp.int32, (n, 1), 0) % prompts
        offset = tot_ref[0:1, :]
        for p in range(1, prompts):
            offset = jnp.where(row_prompt == p, tot_ref[p : p + 1, :], offset)
        qt_ref[rows, :] = (q * jnp.exp(b + offset)).astype(bf16)
        start_query = (q * jnp.exp(b)).astype(bf16)
        end_key = (k * jnp.exp(rest)).astype(bf16)
        near_q0 = (q[:half] * jnp.exp(d0)).astype(bf16)
        near_k0 = (k[:half] * jnp.exp(-d0)).astype(bf16)
        near_q1 = (q[half:] * jnp.exp(d1[half:])).astype(bf16)
        near_k1 = (k * jnp.exp(-d1)).astype(bf16)
        block_total = b[n - prompts :]
        decay = jnp.exp(block_total)
        tot_ref[:prompts, :] = tot_ref[:prompts, :] + block_total
        r_at = lax.broadcasted_iota(jnp.int32, (n, n), 0)
        c_at = lax.broadcasted_iota(jnp.int32, (n, n), 1)
        keep = (c_at <= r_at) & (r_at % prompts == c_at % prompts)
        for h in range(heads):
            kc = slice(h * DK, (h + 1) * DK)
            v = vs[rows, h * DV : (h + 1) * DV]
            w0 = jnp.where(keep[:half, :half], dot_nt(near_q0[:, kc], near_k0[:, kc]), 0.0).astype(bf16)
            w1 = jnp.where(keep[half:], dot_nt(near_q1[:, kc], near_k1[:, kc]), 0.0).astype(bf16)
            inner = jnp.concatenate([dot(w0, v[:half]), dot(w1, v)], axis=0)
            state = st_ref[h]
            from_all = dot_nt(start_query[:, kc], state.astype(bf16))
            from_state = from_all[:, :DV]
            for p in range(1, prompts):
                from_state = jnp.where(row_prompt == p, from_all[:, p * DV : (p + 1) * DV], from_state)
            out_ref[rows, h * DV : (h + 1) * DV] = (inner + from_state).astype(bf16)
            zero = jnp.zeros_like(v)
            v_each = jnp.concatenate([jnp.where(row_prompt == p, v, zero) for p in range(prompts)], axis=1)
            added = dot_tn(v_each, end_key[:, kc])
            for p in range(prompts):
                at = slice(p * DV, (p + 1) * DV)
                st_ref[h, at, :] = state[at] * decay[p : p + 1, kc] + added[at]


def back_kernel(
    own, chunk, prompts, heads,
    out_ref, qt_ref, in_ref, gain_ref, dec_ref, w_hbm,
    y_ref, yd_ref,
    w, nl, nr, dl, dr,
    w_sem, send_sem, recv_sem, dsend, drecv,
):
    me = lax.axis_index("tp")
    other = 1 - me
    count = own // chunk
    load = pltpu.make_async_copy(w_hbm, w, w_sem)
    load.start()
    meet_partner(other)

    def head_norm(part, h):
        factor = lax.rsqrt(jnp.mean(part * part, axis=-1, keepdims=True) + norm_eps)
        return (part * factor * gain_ref[:, h * DV : (h + 1) * DV]).astype(bf16)

    def finish(at):
        rows = pl.ds(pl.multiple_of(at, chunk), chunk)
        row_prompt = lax.broadcasted_iota(jnp.int32, (chunk, 1), 0) % prompts
        for h in range(heads):
            cols = slice(h * DV, (h + 1) * DV)
            from_all = dot_nt(qt_ref[rows, h * DK : (h + 1) * DK], in_ref[h])
            from_state = from_all[:, :DV]
            for p in range(1, prompts):
                from_state = jnp.where(row_prompt == p, from_all[:, p * DV : (p + 1) * DV], from_state)
            nl[rows, cols] = head_norm(out_ref[rows, cols].astype(f32) + from_state, h)

    def copy(j):
        src = pl.ds(pl.multiple_of(other * own + j * chunk, chunk), chunk)
        return pltpu.make_async_remote_copy(
            src_ref=nl.at[src], dst_ref=nr.at[pl.ds(j * chunk, chunk)], send_sem=send_sem.at[j], recv_sem=recv_sem.at[j],
            device_id={"tp": other}, device_id_type=MESH,
        )

    for h in range(heads):
        cols = slice(h * DV, (h + 1) * DV)
        dl[:, cols] = head_norm(dec_ref[:, cols], h)
    dec_copy = pltpu.make_async_remote_copy(
        src_ref=dl.at[pl.ds(pl.multiple_of(other * PAD, PAD), PAD)], dst_ref=dr, send_sem=dsend, recv_sem=drecv,
        device_id={"tp": other}, device_id_type=MESH,
    )
    for j in range(count):
        finish(other * own + j * chunk)
        if j == 0:
            dec_copy.start()
        else:
            copy(j - 1).start()
    finish(me * own)
    copy(count - 1).start()

    if count > 1:
        @pl.loop(1, count)
        def _(j):
            finish(me * own + j * chunk)

    load.wait()
    width = nl.shape[1]
    w_mine = pl.ds(pl.multiple_of(me * width, width), width)
    w_other = pl.ds(pl.multiple_of(other * width, width), width)
    tile = 512
    for j in range(count):
        copy(j).wait_recv()

        @pl.loop(0, w.shape[1] // tile)
        def _(t):
            cols = pl.ds(pl.multiple_of(t * tile, tile), tile)
            held = nl[pl.ds(pl.multiple_of(me * own + j * chunk, chunk), chunk), :]
            y_ref[pl.ds(j * chunk, chunk), cols] = (
                dot(held, w[w_mine, cols]) + dot(nr[pl.ds(j * chunk, chunk), :], w[w_other, cols])
            ).astype(bf16)

    dec_copy.wait()
    held = dl[pl.ds(pl.multiple_of(me * PAD, PAD), PAD), :]
    yd_ref[...] = (dot(held, w[w_mine, :]) + dot(dr[...], w[w_other, :])).astype(bf16)
    for j in range(count):
        copy(j).wait_send()


def decode_kernel(heads, cols_ref, v_ref, s_ref, att_ref, new_ref):
    for h in range(heads):
        state = s_ref[0, h]
        qe = cols_ref[0, :, h : h + 1]
        e = cols_ref[0, :, heads + h : heads + h + 1]
        k = cols_ref[0, :, 2 * heads + h : 2 * heads + h + 1]
        qk = cols_ref[0, 0:1, 3 * heads + h : 3 * heads + h + 1]
        v = v_ref[0, :, h * DV : (h + 1) * DV]
        att_ref[0, :, h * DV : (h + 1) * DV] = jnp.sum(qe * state, axis=0, keepdims=True) + qk * v
        new_ref[0, h] = e * state + k * v


ANY = pl.BlockSpec(memory_space=pl.ANY)
VMEM = pl.BlockSpec(memory_space=pltpu.VMEM)
LIMIT = 60 * 1024 * 1024


def on_device(
    pieces, new_tokens, w_query, w_key, w_value, w_decay, decay_bias, norm_gain, head_gain, w_out, prompt_state, decode_state,
):
    kv_size = lax.axis_size("kv")
    tp_index = lax.axis_index("tp")
    kv_index = lax.axis_index("kv")
    qk = w_query.shape[1]
    heads = qk // DK
    vw = heads * DV
    own_pos, prompts, width = pieces.shape
    own = own_pos * prompts
    chunk = min(256, own)
    count = own // chunk
    rows = 2 * own
    dec_own = new_tokens.shape[0]
    bias_here = lax.dynamic_slice_in_dim(decay_bias, tp_index * qk, qk)[None]
    gain_here = lax.dynamic_slice_in_dim(head_gain, tp_index * vw, vw)[None]
    whole_start = lax.all_gather(prompt_state.astype(bf16), "kv", axis=2, tiled=True)
    whole_start = whole_start.transpose(1, 0, 3, 2).astype(f32)

    mats = jnp.asarray(sum_matrices(prompts), bf16)
    dec_rows = jnp.pad(new_tokens, ((0, PAD - dec_own), (0, 0)))
    proj_flops = 2 * rows * width * (3 * qk + vw)
    out_local, q_total, local, totals, dec_prod = pl.pallas_call(
        functools.partial(front_kernel, own, chunk, prompts, heads),
        name="front",
        out_shape=(
            jax.ShapeDtypeStruct((rows, vw), bf16),
            jax.ShapeDtypeStruct((rows, qk), bf16),
            jax.ShapeDtypeStruct((heads, prompts * DV, DK), f32),
            jax.ShapeDtypeStruct((8, qk), f32),
            jax.ShapeDtypeStruct((2 * PAD, 3 * qk + vw), f32),
        ),
        in_specs=[ANY, VMEM, ANY, ANY, ANY, ANY, VMEM, VMEM, VMEM],
        out_specs=(VMEM,) * 5,
        scratch_shapes=[
            pltpu.VMEM((own, width), bf16),
            pltpu.VMEM((rows, width), bf16),
            pltpu.VMEM((2 * PAD, width), bf16),
            pltpu.VMEM((width, qk), bf16),
            pltpu.VMEM((width, qk), bf16),
            pltpu.VMEM((width, vw), bf16),
            pltpu.VMEM((width, qk), bf16),
            pltpu.VMEM((rows, qk), bf16),
            pltpu.VMEM((rows, qk), bf16),
            pltpu.VMEM((rows, vw), bf16),
            pltpu.VMEM((rows, qk), f32),
            pltpu.SemaphoreType.DMA((count,)),
            pltpu.SemaphoreType.DMA((4,)),
            pltpu.SemaphoreType.DMA((count,)),
            pltpu.SemaphoreType.DMA((count,)),
            pltpu.SemaphoreType.DMA,
            pltpu.SemaphoreType.DMA,
        ],
        compiler_params=pltpu.CompilerParams(collective_id=0, has_side_effects=True, vmem_limit_bytes=LIMIT),
        cost_estimate=pl.CostEstimate(flops=proj_flops, bytes_accessed=20_000_000, transcendentals=0),
    )(pieces.reshape(own, width), dec_rows, w_query, w_key, w_value, w_decay, bias_here, norm_gain[None], mats)

    totals = totals[:prompts].reshape(prompts, heads, DK).transpose(1, 0, 2)[:, :, None]
    local = local.reshape(heads, prompts, DV, DK)
    all_local = lax.all_gather(local.astype(bf16), "kv")
    all_totals = lax.all_gather(totals, "kv")

    dec_all = dec_prod.reshape(2, PAD, -1)[:, :dec_own].reshape(2 * dec_own, -1)
    seqs = 2 * dec_own
    q_d = dec_all[:, :qk].reshape(seqs, heads, DK)
    k_d = dec_all[:, qk : 2 * qk].reshape(seqs, heads, DK)
    e_d = jnp.exp(dec_all[:, 2 * qk : 3 * qk]).reshape(seqs, heads, DK)
    qk_d = jnp.broadcast_to(jnp.sum(q_d * k_d, axis=-1, keepdims=True), q_d.shape)
    cols = jnp.concatenate([q_d * e_d, e_d, k_d, qk_d], axis=1).transpose(0, 2, 1)
    v_d = dec_all[:, 3 * qk :][:, None]
    dec_att, decode_out = pl.pallas_call(
        functools.partial(decode_kernel, heads),
        name="decode",
        grid=(seqs,),
        out_shape=(
            jax.ShapeDtypeStruct((seqs, 1, vw), f32),
            jax.ShapeDtypeStruct(decode_state.shape, f32),
        ),
        in_specs=[
            pl.BlockSpec((1, DK, 4 * heads), lambda i: (i, 0, 0)),
            pl.BlockSpec((1, 1, vw), lambda i: (i, 0, 0)),
            pl.BlockSpec((1, heads, DK, DV), lambda i: (i, 0, 0, 0)),
        ],
        out_specs=(
            pl.BlockSpec((1, 1, vw), lambda i: (i, 0, 0)),
            pl.BlockSpec((1, heads, DK, DV), lambda i: (i, 0, 0, 0)),
        ),
        cost_estimate=pl.CostEstimate(flops=8 * decode_state.size, bytes_accessed=8 * decode_state.size, transcendentals=0),
    )(cols, v_d, decode_state)

    running = whole_start
    incoming = whole_start
    for c in range(kv_size):
        incoming = jnp.where(kv_index == c, running, incoming)
        running = jnp.exp(all_totals[c]) * running + all_local[c].astype(f32)
    rows_k = prompt_state.shape[2]
    prompt_out = lax.dynamic_slice_in_dim(running, kv_index * rows_k, rows_k, 3).transpose(1, 0, 3, 2)

    dec_pad = jnp.pad(dec_att.reshape(2, dec_own, vw), ((0, 0), (0, PAD - dec_own), (0, 0))).reshape(2 * PAD, vw)
    y, yd = pl.pallas_call(
        functools.partial(back_kernel, own, chunk, prompts, heads),
        name="back",
        out_shape=(
            jax.ShapeDtypeStruct((own, w_out.shape[1]), bf16),
            jax.ShapeDtypeStruct((PAD, w_out.shape[1]), bf16),
        ),
        in_specs=[VMEM] * 5 + [ANY],
        out_specs=(VMEM,) * 2,
        scratch_shapes=[
            pltpu.VMEM(w_out.shape, bf16),
            pltpu.VMEM((rows, vw), bf16),
            pltpu.VMEM((own, vw), bf16),
            pltpu.VMEM((2 * PAD, vw), bf16),
            pltpu.VMEM((PAD, vw), bf16),
            pltpu.SemaphoreType.DMA,
            pltpu.SemaphoreType.DMA((count,)),
            pltpu.SemaphoreType.DMA((count,)),
            pltpu.SemaphoreType.DMA,
            pltpu.SemaphoreType.DMA,
        ],
        compiler_params=pltpu.CompilerParams(collective_id=1, has_side_effects=True, vmem_limit_bytes=LIMIT),
        cost_estimate=pl.CostEstimate(flops=2 * own * w_out.size, bytes_accessed=20_000_000, transcendentals=0),
    )(out_local, q_total, incoming.reshape(heads, prompts * DV, DK).astype(bf16), gain_here, dec_pad, w_out)
    return (y.reshape(own_pos, prompts, -1), yd[:dec_own], prompt_out, decode_out)


def solution(mesh):
    return jax.shard_map(
        on_device,
        mesh=mesh,
        in_specs=(
            P(("kv", "tp"), "dp", None),
            P(("dp", "kv", "tp"), None),
            P(None, "tp"),
            P(None, "tp"),
            P(None, "tp"),
            P(None, "tp"),
            P(),
            P(),
            P(),
            P(),
            P("dp", "tp", "kv", None),
            P(("dp", "kv"), "tp", None, None),
        ),
        out_specs=(
            P(("kv", "tp"), "dp", None),
            P(("dp", "kv", "tp"), None),
            P("dp", "tp", "kv", None),
            P(("dp", "kv"), "tp", None, None),
        ),
        check_vma=False,
    )
```

profile of v0, /device:TPU:0, one launch (start us, length us, event | category | flops | bytes accessed | tf_op | source)
XLA Modules:
  0.0 180.9 jit_solution(9294594393646219178)
XLA Ops:
  7.2 0.0 all-gather.3.cloned.1.call-start
  7.2 0.0 copy-start.4
  7.2 0.0 copy-start.1
  7.2 7.2 %reshape.93.x_hbm = bf16[1024,2048]{1,0:T(8,128)(2,1)} reshape(bf16[512,2,2048]{2,1,0:T(2,128)(2,1)} %param.13) | data formatting | bytes 8388608 | tf_op jit(solution)/shard_map/reshape | solution.py:357
  14.4 0.0 copy-done.4
  14.4 0.7 dynamic_slice.9
  15.1 0.0 copy-done.1
  15.1 0.6 pad.8.dec_ref
  15.7 0.0 copy-start
  15.7 59.1 %front.1 = (bf16[2048,1024]{1,0:T(8,128)(2,1)}, bf16[2048,512]{1,0:T(8,128)(2,1)}, f32[4,512,128]{2,1,0:T(8,128)}, f32[8,512]{1,0:T(8,128)}, f32[32,2560]{1,0:T(8,128)}) custom-call(bf16[1024,2048]{1,0:T(8,128)(2,1)} %reshape.93.x_hbm, bf16[16,2048]{1,0:T(8,128)(2,1)} %pad.8.dec_ref, bf16[2048,512]{1,0:T(8,128)(2,1)} %wq_hbm.1, bf16[2048,512]{1,0:T(8,128)(2,1)} %wk_hbm.1, ...), custom_call_target="tpu_custom_call" | custom-call | flops 21474836480 | bytes 20000000 | tf_op jit(solution)/shard_map/front/pallas_call | solution.py:324
  74.8 2.1 %convert_element_type.58 = bf16[4,512,128]{2,1,0:T(8,128)(2,1)} convert(f32[4,512,128]{2,1,0:T(8,128)} %get-tuple-element.16) | non-fusion elementwise | flops 262144 | bytes 1572864 | tf_op jit(solution)/shard_map/convert_element_type | solution.py:361
  76.9 0.0 all-gather.3.cloned.1.call-update
  76.9 0.0 copy-done
  76.9 0.2 copy.72
  77.1 0.7 slice_bitcast_fusion.1
  77.8 15.0 %all-gather = f32[16,2,128]{2,1,0:T(2,128)S(1)} all-gather(f32[4,2,128]{2,1,0:T(2,128)S(1)} %slice_bitcast_fusion.1), channel_id=2, replica_groups=mesh['dp'=4,'kv'=4,'tp'=2] {'kv'}, dimensions={0}, use_global_device_ids=true | all-gather | bytes 20480 | tf_op jit(solution)/shard_map/all_gather | solution.py:362
  92.8 0.2 copy.46
  93.0 0.2 copy.42
  93.2 0.2 copy.54
  93.4 0.2 copy.44
  93.5 0.9 slice_bitcast_fusion
  94.5 0.7 broadcast_in_dim.22.v_ref
  95.3 0.1 fusion.6
  95.4 1.3 copy.52
  96.7 0.0 copy-start.3
  96.7 14.3 %decode.1 = (f32[16,1,1024]{2,1,0:T(1,128)}, f32[16,4,128,256]{3,2,1,0:T(8,128)}) custom-call(f32[16,128,16]{2,1,0:T(8,128)} %bitcast.64, f32[16,1,1024]{2,1,0:T(1,128)} %broadcast_in_dim.22.v_ref, f32[16,4,128,256]{3,2,1,0:T(8,128)} %s_ref.1), custom_call_target="tpu_custom_call" | custom-call | flops 16777216 | bytes 16777216 | tf_op jit(solution)/shard_map/decode/pallas_call | solution.py:372
  111.0 0.9 copy.73
  111.8 0.0 copy-done.3
  111.9 0.6 dynamic_slice.10
  112.5 0.7 pad.9
  113.1 0.6 constant_dynamic-slice_fusion
  113.7 21.5 %all_gather.11 = bf16[2,4,128,256]{3,1,0,2:T(4,128)(2,1)S(1)} all-gather(bf16[2,4,32,256]{3,1,0,2:T(4,128)(2,1)S(1)} %copy.72), channel_id=1, replica_groups=mesh['dp'=4,'kv'=4,'tp'=2] {'kv'}, dimensions={2}, use_global_device_ids=true | all-gather | bytes 655360 | tf_op jit(solution)/shard_map/all_gather | solution.py:318
  135.2 0.0 all-gather.3.cloned.1.call-done
  135.2 1.7 fusion.11
  136.9 0.4 copy.65
  137.3 0.4 copy.63
  137.7 0.4 copy.62
  138.2 0.4 copy.61
  138.6 2.2 %convert_add_fusion = (f32[4,2,256,128]{2,0,1,3:T(4,128)S(1)}, bf16[4,2,256,128]{2,0,1,3:T(4,128)(2,1)S(1)}) fusion(bf16[1,4,2,256,128]{3,1,2,4,0:T(4,128)(2,1)S(1)} %copy.63, bf16[1,4,2,256,128]{3,1,2,4,0:T(4,128)(2,1)S(1)} %copy.62, bf16[2,4,128,256]{3,1,0,2:T(4,128)(2,1)S(1)} %all_gather.11, bf16[1,4,2,256,128]{3,1,2,4,0:T(4,128)(2,1)S(1)} %copy.61, ...), kind=kLoop, calls=%fused_computation | loop fusion | flops 3670016 | bytes 3682307 | tf_op jit(solution)/shard_map/add | solution.py:396
  140.8 0.9 fusion.5
  141.7 0.8 copy.56
  142.5 1.2 copy.51
  143.7 22.0 %back.1 = (bf16[1024,2048]{1,0:T(8,128)(2,1)}, bf16[16,2048]{1,0:T(8,128)(2,1)}) custom-call(bf16[2048,1024]{1,0:T(8,128)(2,1)} %get-tuple-element.13.out_ref, bf16[2048,512]{1,0:T(8,128)(2,1)} %get-tuple-element.14.qt_ref, bf16[4,512,128]{2,1,0:T(8,128)(2,1)} %bitcast.67, f32[1,1024]{1,0:T(1,128)} %bitcast.71, f32[32,1024]{1,0:T(8,128)} %bitcast.69, ...), custom_call_target="tpu_custom_call" | custom-call | flops 8589934592 | bytes 20000000 | tf_op jit(solution)/shard_map/back/pallas_call | solution.py:401
  165.8 0.0 copy-start.2
  165.8 7.6 %reshape.102 = bf16[512,2,2048]{2,1,0:T(2,128)(2,1)} reshape(bf16[1024,2048]{1,0:T(8,128)(2,1)} %get-tuple-element.19) | data formatting | bytes 8388608 | tf_op jit(solution)/shard_map/reshape | solution.py:425
  173.4 0.0 copy-done.2
  173.4 0.6 slice.57
  (11 shorter events, 0.1 us)
Async XLA Ops:
  7.2 128.0 %all-gather.3.cloned.1.call-start = ((), (), s32[]{:S(2)}) async-start(), calls=%async_computation | async-start | bytes 2621440 | tf_op jit(solution)/shard_map/all_gather | solution.py:361
  7.2 7.2 %copy-start.4 = (f32[1024]{0:T(1024)S(1)}, f32[1024]{0:T(1024)}, u32[]{:S(2)}) copy-start(f32[1024]{0:T(1024)} %param.19) | copy-start | bytes 12292
  7.2 7.8 %copy-start.1 = (bf16[8,2048]{1,0:T(8,128)(2,1)S(1)}, bf16[8,2048]{1,0:T(8,128)(2,1)}, u32[]{:S(2)}) copy-start(bf16[8,2048]{1,0:T(8,128)(2,1)} %param.14) | copy-start | bytes 98308
  15.7 61.2 %copy-start = (f32[2,4,32,256]{3,2,1,0:T(8,128)S(1)}, f32[2,4,32,256]{3,2,1,0:T(8,128)}, u32[]{:S(2)}) copy-start(f32[2,4,32,256]{3,2,1,0:T(8,128)} %param.23) | copy-start | bytes 786436
  96.7 15.1 %copy-start.3 = (f32[2048]{0:T(1024)S(1)}, f32[2048]{0:T(1024)}, u32[]{:S(2)}) copy-start(f32[2048]{0:T(1024)} %param.21) | copy-start | bytes 24580
  165.8 7.7 %copy-start.2 = (bf16[16,2048]{1,0:T(8,128)(2,1)S(1)}, bf16[16,2048]{1,0:T(8,128)(2,1)}, u32[]{:S(2)}) copy-start(bf16[16,2048]{1,0:T(8,128)(2,1)} %get-tuple-element.20) | copy-start | bytes 196612
Sparse Core Ops, SparseCore 0:
  77.0 55.9 all-gather.2
where the time goes:
time: 182 us; the launch traced here: 181 us
  Pallas kernels  95.4 us (52%)
  blocking collectives  36.5 us (20%)
  local copies, waits for them, and re-layouts  29.4 us (16%)
  between operations  14.3 us (8%)
  other arithmetic  5.34 us (3%)
    pallas_call x1, Pallas kernels, on_device(): pl.pallas_call(functools.partial(front_kernel, own, chunk, prompts, heads...  59.1 us
    pallas_call x1, Pallas kernels, on_device(): pl.pallas_call(functools.partial(back_kernel, own, chunk, prompts, heads)...  22 us
    all_gather x1, blocking collectives, on_device(): lax.all_gather(prompt_state.astype(bf16), 'kv', axis=2, tiled=True)  21.5 us
    all_gather x1, blocking collectives, on_device(): all_totals = lax.all_gather(totals, 'kv')  15 us
    pallas_call x1, Pallas kernels, on_device(): pl.pallas_call(functools.partial(decode_kernel, heads), name='decode', gr...  14.3 us
    reshape x1, local copies, waits for them, and re-layouts, on_device(): y.reshape(own_pos, prompts, -1)  7.65 us
    reshape x1, local copies, waits for them, and re-layouts, on_device(): pieces.reshape(own, width)  7.18 us
  transfers between devices with their start and end apart: 1, of which 0 were waited for; matrix products, arithmetic and copies ran while one was open for 4% of the time, Pallas kernels for 8%

commit v1 on v0

v1 whole, which is shorter than its diff:
```python
import functools

import jax
import jax.numpy as jnp
import numpy as np
from jax import lax
from jax.experimental import pallas as pl
from jax.experimental.pallas import tpu as pltpu
from jax.sharding import PartitionSpec as P

DK = 128
DV = 256
STEP = 64
PART = 16

norm_eps = 0.1
decay_tau = 16.0
f32, bf16 = jnp.float32, jnp.bfloat16
MESH = pl.DeviceIdType.MESH
PAD = 16


def dot(a, b):
    return jnp.dot(a, b, preferred_element_type=f32)


def dot_nt(a, b):
    return lax.dot_general(a, b, (((1,), (1,)), ((), ())), preferred_element_type=f32)


def dot_tn(a, b):
    return lax.dot_general(a, b, (((0,), (0,)), ((), ())), preferred_element_type=f32)


def sum_matrices(prompts):
    n = STEP * prompts
    r, c = np.arange(n)[:, None], np.arange(n)[None]
    same = (r % prompts) == (c % prompts)

    def from_anchor(edge):
        return (same & (c >= edge) & (c <= r)) * 1.0 - (same & (c < edge) & (c > r)) * 1.0

    b = (same & (c <= r)) * 1.0
    rest = (same & (c > r)) * 1.0
    whole = ((np.arange(16)[:, None] == (c % prompts))) * 1.0
    d0 = from_anchor(PART * prompts)[: n // 2]
    d1 = from_anchor(3 * PART * prompts)
    for_keys = np.concatenate([rest, whole], axis=0)
    near = np.concatenate([b, d0, d1], axis=0)
    return np.concatenate([for_keys] * 2, axis=1), np.concatenate([near] * 2, axis=1)


def normed(rows, gain):
    wide = rows.astype(f32)
    factor = lax.rsqrt(jnp.mean(wide * wide, axis=-1, keepdims=True) + norm_eps)
    return wide * factor * gain


def halves(g):
    hi = g.astype(bf16)
    mid = (g - hi.astype(f32)).astype(bf16)
    return jnp.concatenate([hi, mid], axis=0)


def each_prompt(rows, prompts):
    row_prompt = lax.broadcasted_iota(jnp.int32, (rows.shape[0], 1), 0) % prompts
    zero = jnp.zeros_like(rows)
    return jnp.concatenate([jnp.where(row_prompt == p, rows, zero) for p in range(prompts)], axis=1)


def by_prompt(table, row_prompt, prompts):
    picked = table[0:1]
    for p in range(1, prompts):
        picked = jnp.where(row_prompt == p, table[p : p + 1], picked)
    return picked


def main_kernel(
    own_pos, prompts, heads, kv, dec_own,
    x_hbm, dec_ref, wq_hbm, wk_hbm, wv_hbm, wd_hbm, bias_ref, gain_ref, head_gain_ref, mk_ref, mq_ref, ps_ref, ds_hbm,
    nrm_hbm, ndec_hbm, po_ref, cols_ref, vrow_ref,
    xb, nb, nd, wq, wk, wv, wd, qs, ks, vs, gs, sq, ek, es, oi, tots, later, st, loc, rx, inc, sin, tb, rxt, ttr,
    sbuf, qet, attb, dl,
    x_sem, w_sem, n_send, n_recv, nd_send, nd_recv, p1_send, p1_recv, t_send, t_recv, p2_send, p2_recv,
    s_sem, out_local, out_send, out_recv, d_local, d_send, d_recv,
):
    me = lax.axis_index("tp")
    other = 1 - me
    here = lax.axis_index("kv")
    own = own_pos * prompts
    rows_all = 2 * own
    chunk = min(256, own)
    count = own // chunk
    n = STEP * prompts
    half = n // 2
    blocks = rows_all // n
    group = 2 if heads % 2 == 0 else 1
    groups = heads // group
    gk, gv = group * DK, group * DV
    qk, vw = heads * DK, heads * DV
    part = DK // kv
    seqs = 2 * dec_own
    pos = chunk // prompts

    def x_copy(j):
        at = pl.ds(j * pos, pos)
        return pltpu.make_async_copy(x_hbm.at[at], xb.at[at], x_sem.at[j])

    for j in range(count):
        x_copy(j).start()
    loads = []
    for i in range(groups):
        kc, vc = pl.ds(i * gk, gk), pl.ds(i * gv, gv)
        for s, (src, dst, cols) in enumerate(((wk_hbm, wk, kc), (wd_hbm, wd, kc), (wv_hbm, wv, vc))):
            loads.append(pltpu.make_async_copy(src.at[:, cols], dst.at[:, cols], w_sem.at[3 * i + s]))
    loads.append(pltpu.make_async_copy(wq_hbm, wq, w_sem.at[3 * groups]))
    for load in loads:
        load.start()

    barrier = pltpu.get_barrier_semaphore()
    pl.semaphore_signal(barrier, inc=1, device_id={"tp": other}, device_id_type=MESH)
    for d in range(1, kv):
        pl.semaphore_signal(barrier, inc=1, device_id={"kv": lax.rem(here + d, kv)}, device_id_type=MESH)
    pl.semaphore_wait(barrier, kv)

    def state_copy(h):
        return pltpu.make_async_copy(ds_hbm.at[:, h], sbuf.at[h % 2], s_sem.at[h])

    def piece_copy(j, side):
        rows = pl.ds(pl.multiple_of(side * own + j * chunk, chunk), chunk)
        return pltpu.make_async_remote_copy(
            src_ref=nb.at[rows], dst_ref=nb.at[rows], send_sem=n_send.at[j], recv_sem=n_recv.at[j],
            device_id={"tp": other}, device_id_type=MESH,
        )

    mine = pl.ds(pl.multiple_of(me * PAD, PAD), PAD)
    theirs = pl.ds(pl.multiple_of(other * PAD, PAD), PAD)
    dec_rows = normed(dec_ref[...], gain_ref[...])
    nd[mine, :] = jnp.concatenate([dec_rows, jnp.zeros((PAD - dec_own, dec_rows.shape[1]), f32)], axis=0).astype(bf16)
    dec_copy = pltpu.make_async_remote_copy(
        src_ref=nd.at[mine], dst_ref=nd.at[mine], send_sem=nd_send, recv_sem=nd_recv,
        device_id={"tp": other}, device_id_type=MESH,
    )
    small = min(32, pos)
    for j in range(count):
        x_copy(j).wait()

        @pl.loop(0, pos // small)
        def _(s):
            at = pl.multiple_of(j * pos + s * small, small)
            rows = xb[pl.ds(at, small)].reshape(small * prompts, xb.shape[2])
            to = pl.ds(pl.multiple_of(me * own + at * prompts, small * prompts), small * prompts)
            nb[to, :] = normed(rows, gain_ref[...]).astype(bf16)

        if j == 0:
            dec_copy.start()
        else:
            piece_copy(j - 1, me).start()
    piece_copy(count - 1, me).start()

    def decay_of(product, i):
        at = pl.ds(pl.multiple_of(me * qk + i * gk, gk), product.shape[1])
        t = product + bias_ref[:, at]
        return (jnp.minimum(t, 0.0) - jnp.log1p(jnp.exp(-jnp.abs(t)))) * (1.0 / decay_tau)

    def project(at, i):
        rows = pl.ds(pl.multiple_of(at, chunk), chunk)
        kc, vc = slice(i * gk, (i + 1) * gk), slice(i * gv, (i + 1) * gv)
        block = nb[rows, :]
        ks[rows, kc] = dot(block, wk[:, kc]).astype(bf16)
        vs[rows, vc] = dot(block, wv[:, vc]).astype(bf16)
        gs[rows, kc] = decay_of(dot(block, wd[:, kc]), i)

    row_prompt = lax.broadcasted_iota(jnp.int32, (n, 1), 0) % prompts

    def keys_of(i):
        kc = slice(i * gk, (i + 1) * gk)
        later[:, kc] = jnp.zeros((8, gk), f32)

        @pl.loop(0, blocks)
        def _(back):
            at = blocks - 1 - back
            rows = pl.ds(pl.multiple_of(at * n, n), n)
            sums = dot(mk_ref[...], halves(gs[rows, kc]))
            end = ks[rows, kc].astype(f32) * jnp.exp(sums[:n])
            ek[rows, kc] = end.astype(bf16)
            after = later[:, kc]
            es[rows, :] = (end * by_prompt(jnp.exp(after), row_prompt, prompts)).astype(bf16)
            total = sums[n : n + 8]
            tots[at, :, kc] = total
            later[:, kc] = after + total

        span = min(512, rows_all)
        for hh in range(group):
            h = i * group + hh
            hk, hv = slice(hh * DK, (hh + 1) * DK), slice(h * DV, (h + 1) * DV)
            st[h] = jnp.zeros(st.shape[1:], f32)

            @pl.loop(0, rows_all // span)
            def _(c):
                rows = pl.ds(pl.multiple_of(c * span, span), span)
                st[h] = st[h] + dot_tn(each_prompt(es[rows, hk], prompts), vs[rows, hv])

            for p in range(prompts):
                loc[h * prompts + p] = st[h, p * DK : (p + 1) * DK, :].astype(bf16)
                tb[i, hh * prompts + p : hh * prompts + p + 1, :] = later[p : p + 1, h * DK : (h + 1) * DK]
            for d in range(1, kv):
                local_copy(d, h).start()
        for d in range(1, kv):
            total_copy(d, i).start()

    def local_copy(d, h):
        to = lax.rem(here + d, kv)
        hp = pl.ds(h * prompts, prompts)
        return pltpu.make_async_remote_copy(
            src_ref=loc.at[hp, pl.ds(pl.multiple_of(to * part, part), part)], dst_ref=rx.at[d, hp],
            send_sem=p1_send.at[d, h], recv_sem=p1_recv.at[d, h], device_id={"kv": to}, device_id_type=MESH,
        )

    def total_copy(d, i):
        return pltpu.make_async_remote_copy(
            src_ref=tb.at[i], dst_ref=rxt.at[d, i], send_sem=t_send.at[d, i], recv_sem=t_recv.at[d, i],
            device_id={"kv": lax.rem(here + d, kv)}, device_id_type=MESH,
        )

    def incoming_copy(d, i):
        to = lax.rem(here + d, kv)
        hp = pl.ds(i * group * prompts, group * prompts)
        return pltpu.make_async_remote_copy(
            src_ref=inc.at[to, hp], dst_ref=sin.at[hp, pl.ds(pl.multiple_of(here * part, part), part)],
            send_sem=p2_send.at[d, i], recv_sem=p2_recv.at[d, i], device_id={"kv": to}, device_id_type=MESH,
        )

    my_part = pl.ds(pl.multiple_of(here * part, part), part)

    def pass_on(i):
        for d in range(1, kv):
            total_copy(d, i).wait_recv()
            for hh in range(group):
                local_copy(d, i * group + hh).wait_recv()
        rxt[0, i] = tb[i]
        for hh in range(group):
            for p in range(prompts):
                hp = (i * group + hh) * prompts + p
                rx[0, hp] = loc[hp, my_part, :]
        for c in range(kv):
            d = lax.rem(here - c + kv, kv)
            ttr[c] = jnp.transpose(jnp.exp(rxt[d, i]))
        for hh in range(group):
            h = i * group + hh
            for p in range(prompts):
                hp = h * prompts + p
                running = ps_ref[p, h]
                for c in range(kv):
                    d = lax.rem(here - c + kv, kv)
                    inc[c, hp] = running.astype(bf16)
                    at = hh * prompts + p
                    running = running * ttr[c, my_part, at : at + 1] + rx[d, hp].astype(f32)
                po_ref[p, h] = running
        for d in range(1, kv):
            incoming_copy(d, i).start()
        for hh in range(group):
            for p in range(prompts):
                hp = (i * group + hh) * prompts + p
                sin[hp, my_part, :] = inc[here, hp]

    for i in range(groups):
        for s in range(3):
            loads[3 * i + s].wait()
        if i == 0:
            @pl.loop(0, count)
            def _(j):
                project(me * own + j * chunk, 0)

            @pl.loop(0, count)
            def _(j):
                piece_copy(j, other).wait_recv()
                project(other * own + j * chunk, 0)

            for h in range(min(2, heads)):
                state_copy(h).start()
        else:
            @pl.loop(0, 2 * count)
            def _(j):
                project(j * chunk, i)
        keys_of(i)

    loads[3 * groups].wait()

    @pl.loop(0, 2 * count)
    def _(j):
        rows = pl.ds(pl.multiple_of(j * chunk, chunk), chunk)
        qs[rows, :] = (dot(nb[rows, :], wq[...]) * DK ** (-0.5)).astype(bf16)

    for j in range(count):
        piece_copy(j, me).wait_send()
    dec_copy.wait()

    r_at = lax.broadcasted_iota(jnp.int32, (n, n), 0)
    c_at = lax.broadcasted_iota(jnp.int32, (n, n), 1)

    def inside(block):
        rows = pl.ds(pl.multiple_of(block * n, n), n)
        keep = (c_at <= r_at) & (r_at % prompts == c_at % prompts)
        for i in range(groups):
            kc = slice(i * gk, (i + 1) * gk)
            sums = dot(mq_ref[...], halves(gs[rows, kc]))
            b, d0, d1 = sums[:n], sums[n : n + half], sums[n + half :]
            q = qs[rows, kc].astype(f32)
            k = ks[rows, kc].astype(f32)
            sq[rows, kc] = (q * jnp.exp(b)).astype(bf16)
            near_q0 = (q[:half] * jnp.exp(d0)).astype(bf16)
            near_k0 = (k[:half] * jnp.exp(-d0)).astype(bf16)
            near_q1 = (q[half:] * jnp.exp(d1[half:])).astype(bf16)
            near_k1 = (k * jnp.exp(-d1)).astype(bf16)
            for hh in range(group):
                hk = slice(hh * DK, (hh + 1) * DK)
                hv = slice((i * group + hh) * DV, (i * group + hh + 1) * DV)
                v = vs[rows, hv]
                w0 = jnp.where(keep[:half, :half], dot_nt(near_q0[:, hk], near_k0[:, hk]), 0.0).astype(bf16)
                w1 = jnp.where(keep[half:], dot_nt(near_q1[:, hk], near_k1[:, hk]), 0.0).astype(bf16)
                oi[rows, hv] = jnp.concatenate([dot(w0, v[:half]), dot(w1, v)], axis=0).astype(bf16)

    pass_on(0)

    @pl.loop(0, blocks // 2)
    def _(block):
        inside(block)

    for i in range(1, groups):
        pass_on(i)

    @pl.loop(blocks // 2, blocks)
    def _(block):
        inside(block)

    def head_norm(block, h):
        factor = lax.rsqrt(jnp.mean(block * block, axis=-1, keepdims=True) + norm_eps)
        at = pl.ds(pl.multiple_of(me * vw + h * DV, DV), DV)
        return (block * factor * head_gain_ref[:, at]).astype(bf16)

    new = nd[...]
    q_d = (dot(new, wq[...]) * DK ** (-0.5)).astype(bf16).astype(f32)
    k_d = dot(new, wk[...]).astype(bf16).astype(f32)
    e_d = jnp.exp(decay_of(dot(new, wd[...]), 0))
    vrow_ref[...] = dot(new, wv[...]).astype(bf16).astype(f32)
    for h in range(heads):
        at = slice(h * DK, (h + 1) * DK)
        qet[h] = jnp.transpose(q_d[:, at] * e_d[:, at])
        cols_ref[0, h] = jnp.transpose(e_d[:, at])
        cols_ref[1, h] = jnp.transpose(k_d[:, at])
    attb[...] = jnp.zeros_like(attb)
    for h in range(heads):
        state_copy(h).wait()
        for s in range(seqs):
            row = (s // dec_own) * PAD + s % dec_own
            attb[row : row + 1, h * DV : (h + 1) * DV] = jnp.sum(
                sbuf[h % 2, s] * qet[h, :, row : row + 1], axis=0, keepdims=True
            )
        if h + 2 < heads:
            state_copy(h + 2).start()
    for h in range(heads):
        at, hv = slice(h * DK, (h + 1) * DK), slice(h * DV, (h + 1) * DV)
        score = jnp.sum(q_d[:, at] * k_d[:, at], axis=-1, keepdims=True)
        dl[:, hv] = head_norm(attb[:, hv] + score * vrow_ref[:, hv], h)
    my_cols = pl.ds(pl.multiple_of(me * vw, vw), vw)
    dec_keep = pltpu.make_async_copy(dl.at[mine], ndec_hbm.at[:, my_cols], d_local)
    dec_keep.start()
    dec_give = pltpu.make_async_remote_copy(
        src_ref=dl.at[theirs], dst_ref=ndec_hbm.at[:, my_cols], send_sem=d_send, recv_sem=d_recv,
        device_id={"tp": other}, device_id_type=MESH,
    )
    dec_give.start()

    def out_refs(side, j, i):
        rows = pl.ds(pl.multiple_of(side * own + j * n, n), n)
        cols = pl.ds(pl.multiple_of(me * vw + i * gv, gv), gv)
        return oi.at[rows, pl.ds(i * gv, gv)], nrm_hbm.at[pl.ds(pl.multiple_of(j * n, n), n), cols]

    def keep_copy(j, i):
        src, dst = out_refs(me, j, i)
        return pltpu.make_async_copy(src, dst, out_local.at[i, j])

    def give_copy(j, i):
        src, dst = out_refs(other, j, i)
        return pltpu.make_async_remote_copy(
            src_ref=src, dst_ref=dst, send_sem=out_send.at[i, j], recv_sem=out_recv.at[i, j],
            device_id={"tp": other}, device_id_type=MESH,
        )

    for i in range(groups):
        for d in range(1, kv):
            incoming_copy(d, i).wait_recv()
        for hh in range(group):
            h = i * group + hh
            for p in range(prompts):
                st[h, p * DK : (p + 1) * DK, :] = sin[h * prompts + p].astype(f32)

        @pl.loop(0, blocks)
        def _(block):
            rows = pl.ds(pl.multiple_of(block * n, n), n)
            for hh in range(group):
                h = i * group + hh
                hk, hv = slice(h * DK, (h + 1) * DK), slice(h * DV, (h + 1) * DV)
                state = st[h]
                from_state = dot(each_prompt(sq[rows, hk], prompts), state.astype(bf16))
                oi[rows, hv] = head_norm(oi[rows, hv].astype(f32) + from_state, h)
                added = dot_tn(each_prompt(ek[rows, hk], prompts), vs[rows, hv])
                decay = jnp.transpose(jnp.exp(tots[block, :, hk]))
                for p in range(prompts):
                    at = slice(p * DK, (p + 1) * DK)
                    st[h, at, :] = state[at] * decay[:, p : p + 1] + added[at]
            side = block // (blocks // 2)
            j = block - side * (blocks // 2)

            @pl.when(side == me)
            def _():
                keep_copy(j, i).start()

            @pl.when(side != me)
            def _():
                give_copy(j, i).start()

    for d in range(1, kv):
        for h in range(heads):
            local_copy(d, h).wait_send()
        for i in range(groups):
            total_copy(d, i).wait_send()
            incoming_copy(d, i).wait_send()
    dec_keep.wait()
    dec_give.wait()
    for i in range(groups):
        @pl.loop(0, blocks // 2)
        def _(j):
            keep_copy(j, i).wait()
            give_copy(j, i).wait_send()
            give_copy(j, i).wait_recv()


def last_kernel(
    own_pos, prompts, heads, dec_own,
    nrm_hbm, ndec_ref, w_hbm, ds_hbm, cols_ref, vrow_ref, ps_ref,
    y_hbm, yd_ref, po_ref, do_hbm,
    nrm, w, yb, sb,
    n_sem, w_sem, s_sem, y_sem, o_sem,
):
    own = own_pos * prompts
    chunk = min(256, own)
    count = own // chunk
    pos = chunk // prompts
    width = w.shape[1]
    tile = width // heads
    seqs = 2 * dec_own

    def n_copy(j):
        at = pl.ds(j * chunk, chunk)
        return pltpu.make_async_copy(nrm_hbm.at[at], nrm.at[at], n_sem.at[j])

    def w_copy(t):
        at = pl.ds(t * tile, tile)
        return pltpu.make_async_copy(w_hbm.at[:, at], w.at[:, at], w_sem.at[t])

    def s_copy(h):
        return pltpu.make_async_copy(ds_hbm.at[:, h], sb.at[h], s_sem.at[h])

    def o_copy(h):
        return pltpu.make_async_copy(sb.at[h], do_hbm.at[:, h], o_sem.at[h])

    def y_copy(t):
        at = pl.ds(t * tile, tile)
        return pltpu.make_async_copy(yb.at[:, :, at], y_hbm.at[:, :, at], y_sem.at[t])

    n_copy(0).start()
    w_copy(0).start()
    for j in range(1, count):
        n_copy(j).start()
    s_copy(0).start()
    for t in range(1, heads):
        w_copy(t).start()
        s_copy(t).start()
    po_ref[...] = ps_ref[...]
    for t in range(heads):
        at = slice(t * tile, (t + 1) * tile)
        w_copy(t).wait()
        s_copy(t).wait()
        each = -(-seqs // count)
        for j in range(count):
            if t == 0:
                n_copy(j).wait()
            block = dot(nrm[j * chunk : (j + 1) * chunk, :], w[:, at]).astype(bf16)
            yb[j * pos : (j + 1) * pos, :, at] = block.reshape(pos, prompts, tile)
            for s in range(j * each, min(seqs, (j + 1) * each)):
                row = (s // dec_own) * PAD + s % dec_own
                v = vrow_ref[row : row + 1, t * DV : (t + 1) * DV]
                sb[t, s] = sb[t, s] * cols_ref[0, t, :, row : row + 1] + cols_ref[1, t, :, row : row + 1] * v
        yd_ref[:, at] = dot(ndec_ref[...], w[:, at])[:dec_own].astype(bf16)
        y_copy(t).start()
        o_copy(t).start()
    for t in range(heads):
        y_copy(t).wait()
        o_copy(t).wait()


ANY = pl.BlockSpec(memory_space=pl.ANY)
VMEM = pl.BlockSpec(memory_space=pltpu.VMEM)
LIMIT = 62 * 1024 * 1024


def on_device(
    pieces, new_tokens, w_query, w_key, w_value, w_decay, decay_bias, norm_gain, head_gain, w_out, prompt_state, decode_state,
):
    kv = lax.axis_size("kv")
    qk = w_query.shape[1]
    heads = qk // DK
    vw = heads * DV
    own_pos, prompts, width = pieces.shape
    own = own_pos * prompts
    chunk = min(256, own)
    count = own // chunk
    rows = 2 * own
    blocks = rows // (STEP * prompts)
    dec_own = new_tokens.shape[0]
    seqs = 2 * dec_own
    part = DK // kv
    group = 2 if heads % 2 == 0 else 1
    groups = heads // group
    hp = heads * prompts
    mk, mq = (jnp.asarray(m, bf16) for m in sum_matrices(prompts))
    dma = pltpu.SemaphoreType.DMA
    nrm, ndec, prompt_out, cols, v_rows = pl.pallas_call(
        functools.partial(main_kernel, own_pos, prompts, heads, kv, dec_own),
        name="layer",
        out_shape=(
            jax.ShapeDtypeStruct((own, 2 * vw), bf16),
            jax.ShapeDtypeStruct((PAD, 2 * vw), bf16),
            jax.ShapeDtypeStruct(prompt_state.shape, f32),
            jax.ShapeDtypeStruct((2, heads, DK, 2 * PAD), f32),
            jax.ShapeDtypeStruct((2 * PAD, vw), f32),
        ),
        in_specs=[ANY, VMEM, ANY, ANY, ANY, ANY, VMEM, VMEM, VMEM, VMEM, VMEM, VMEM, ANY],
        out_specs=(ANY, ANY, VMEM, VMEM, VMEM),
        scratch_shapes=[
            pltpu.VMEM(pieces.shape, bf16),
            pltpu.VMEM((rows, width), bf16),
            pltpu.VMEM((2 * PAD, width), bf16),
            pltpu.VMEM((width, qk), bf16),
            pltpu.VMEM((width, qk), bf16),
            pltpu.VMEM((width, vw), bf16),
            pltpu.VMEM((width, qk), bf16),
            pltpu.VMEM((rows, qk), bf16),
            pltpu.VMEM((rows, qk), bf16),
            pltpu.VMEM((rows, vw), bf16),
            pltpu.VMEM((rows, qk), f32),
            pltpu.VMEM((rows, qk), bf16),
            pltpu.VMEM((rows, qk), bf16),
            pltpu.VMEM((rows, group * DK), bf16),
            pltpu.VMEM((rows, vw), bf16),
            pltpu.VMEM((blocks, 8, qk), f32),
            pltpu.VMEM((8, qk), f32),
            pltpu.VMEM((heads, prompts * DK, DV), f32),
            pltpu.VMEM((hp, DK, DV), bf16),
            pltpu.VMEM((kv, hp, part, DV), bf16),
            pltpu.VMEM((kv, hp, part, DV), bf16),
            pltpu.VMEM((hp, DK, DV), bf16),
            pltpu.VMEM((groups, 8, DK), f32),
            pltpu.VMEM((kv, groups, 8, DK), f32),
            pltpu.VMEM((kv, DK, 8), f32),
            pltpu.VMEM((2, seqs, DK, DV), f32),
            pltpu.VMEM((heads, DK, 2 * PAD), f32),
            pltpu.VMEM((2 * PAD, vw), f32),
            pltpu.VMEM((2 * PAD, vw), bf16),
            dma((count,)),
            dma((3 * groups + 1,)),
            dma((count,)),
            dma((count,)),
            dma,
            dma,
            dma((kv, heads)),
            dma((kv, heads)),
            dma((kv, groups)),
            dma((kv, groups)),
            dma((kv, groups)),
            dma((kv, groups)),
            dma((heads,)),
            dma((groups, blocks // 2)),
            dma((groups, blocks // 2)),
            dma((groups, blocks // 2)),
            dma,
            dma,
            dma,
        ],
        compiler_params=pltpu.CompilerParams(collective_id=0, has_side_effects=True, vmem_limit_bytes=LIMIT),
    )(
        pieces, new_tokens, w_query, w_key, w_value, w_decay, decay_bias[None], norm_gain[None], head_gain[None],
        mk, mq, prompt_state, decode_state,
    )
    return pl.pallas_call(
        functools.partial(last_kernel, own_pos, prompts, heads, dec_own),
        name="last",
        out_shape=(
            jax.ShapeDtypeStruct(pieces.shape, bf16),
            jax.ShapeDtypeStruct(new_tokens.shape, bf16),
            jax.ShapeDtypeStruct(prompt_state.shape, f32),
            jax.ShapeDtypeStruct(decode_state.shape, f32),
        ),
        in_specs=[ANY, VMEM, ANY, ANY, VMEM, VMEM, VMEM],
        out_specs=(ANY, VMEM, VMEM, ANY),
        scratch_shapes=[
            pltpu.VMEM((own, 2 * vw), bf16),
            pltpu.VMEM(w_out.shape, bf16),
            pltpu.VMEM(pieces.shape, bf16),
            pltpu.VMEM((heads, seqs, DK, DV), f32),
            dma((count,)),
            dma((heads,)),
            dma((heads,)),
            dma((heads,)),
            dma((heads,)),
        ],
        compiler_params=pltpu.CompilerParams(vmem_limit_bytes=LIMIT),
    )(nrm, ndec, w_out, decode_state, cols, v_rows, prompt_out)


def solution(mesh):
    return jax.shard_map(
        on_device,
        mesh=mesh,
        in_specs=(
            P(("kv", "tp"), "dp", None),
            P(("dp", "kv", "tp"), None),
            P(None, "tp"),
            P(None, "tp"),
            P(None, "tp"),
            P(None, "tp"),
            P(),
            P(),
            P(),
            P(),
            P("dp", "tp", "kv", None),
            P(("dp", "kv"), "tp", None, None),
        ),
        out_specs=(
            P(("kv", "tp"), "dp", None),
            P(("dp", "kv", "tp"), None),
            P("dp", "tp", "kv", None),
            P(("dp", "kv"), "tp", None, None),
        ),
        check_vma=False,
    )
```

time: 182 us -> 109 us (0.60)
  blocking collectives: 36.5 us -> 0 us
  local copies, waits for them, and re-layouts: 29.4 us -> 0 us
  between operations: 14.3 us -> 0.8 us
  Pallas kernels: 95.4 us -> 108 us
  other arithmetic: 5.34 us -> 0 us
    all_gather x2 -> x0, blocking collectives: 36.5 us -> none  [the longest x1 21.5 us: on_device(): lax.all_gather(prompt_state.astype(bf16), 'kv', axis=2, tiled=True)]
    reshape x6 -> x0, local copies, waits for them, and re-layouts: 15.8 us -> none  [the longest x1 7.65 us: on_device(): y.reshape(own_pos, prompts, -1)]
    pallas_call x3 -> x2, Pallas kernels: 95.4 us -> 108 us  [the longest x1 89.7 us: on_device(): pl.pallas_call(functools.partial(main_kernel, own_pos, prompts, heads, kv...]
    unnamed x17 -> x0, local copies, waits for them, and re-layouts: 3.55 us -> none
    slice x4 -> x0, local copies, waits for them, and re-layouts: 2.28 us -> none  [the longest x2 1.66 us: on_device(): running = jnp.exp(all_totals[c]) * running + all_local[c].astype(f32)]
    add x1 -> x0, other arithmetic: 2.2 us -> none  [on_device(): running = jnp.exp(all_totals[c]) * running + all_local[c].astype(f32)]
    convert_element_type x1 -> x0, other arithmetic: 2.09 us -> none  [on_device(): all_local = lax.all_gather(local.astype(bf16), 'kv')]
    dynamic_slice x3 -> x0, local copies, waits for them, and re-layouts: 1.86 us -> none  [the longest x1 0.65 us: on_device(): bias_here = lax.dynamic_slice_in_dim(decay_bias, tp_index * qk, qk)[None]]
  transfers between devices with their start and end apart: 1 -> 0, of which waited for: 0 -> 0; matrix products, arithmetic and copies ran while one was open for 4% -> 0% of each run, Pallas kernels for 8% -> 0%
where the time goes in v1:
time: 109 us
  Pallas kernels  108 us (99%)
    pallas_call x1, Pallas kernels, on_device(): pl.pallas_call(functools.partial(main_kernel, own_pos, prompts, heads, kv...  89.7 us
    pallas_call x1, Pallas kernels, on_device(): pl.pallas_call(functools.partial(last_kernel, own_pos, prompts, heads, de...  18.2 us

profile of v1, /device:TPU:0, one launch (start us, length us, event | category | flops | bytes accessed | tf_op | source)
XLA Modules:
  0.0 108.7 jit_solution(5537939890594750836)
XLA Ops:
  0.6 89.7 %layer.1 = (bf16[1024,2048]{1,0:T(8,128)(2,1)}, bf16[16,2048]{1,0:T(8,128)(2,1)}, f32[2,4,32,256]{3,2,1,0:T(8,128)}, f32[2,4,128,32]{3,2,1,0:T(8,128)}, f32[32,1024]{1,0:T(8,128)}) custom-call(bf16[512,2,2048]{2,1,0:T(2,128)(2,1)} %x_hbm.1, bf16[8,2048]{1,0:T(8,128)(2,1)} %dec_ref.1, bf16[2048,512]{1,0:T(8,128)(2,1)} %wq_hbm.1, bf16[2048,512]{1,0:T(8,128)(2,1)} %wk_hbm.1, ...), custom_call_target="tpu_custom_call" | custom-call | tf_op jit(solution)/shard_map/layer/pallas_call | solution.py:530
  90.4 18.2 %last.1 = (bf16[512,2,2048]{2,1,0:T(2,128)(2,1)}, bf16[8,2048]{1,0:T(8,128)(2,1)}, f32[2,4,32,256]{3,2,1,0:T(8,128)}, f32[16,4,128,256]{3,2,1,0:T(8,128)}) custom-call(bf16[1024,2048]{1,0:T(8,128)(2,1)} %get-tuple-element.9.nrm_hbm, bf16[16,2048]{1,0:T(8,128)(2,1)} %get-tuple-element.10.ndec_ref, bf16[2048,2048]{1,0:T(8,128)(2,1)} %w_hbm.1, ...), custom_call_target="tpu_custom_call" | custom-call | tf_op jit(solution)/shard_map/last/pallas_call | solution.py:597

commit v2 on v1

--- a/solution.py
+++ b/solution.py
@@ -66,6 +66,13 @@
     row_prompt = lax.broadcasted_iota(jnp.int32, (rows.shape[0], 1), 0) % prompts
     zero = jnp.zeros_like(rows)
     return jnp.concatenate([jnp.where(row_prompt == p, rows, zero) for p in range(prompts)], axis=1)
+
+
+def turned(rows, prompts):
+    columns = jnp.transpose(rows)
+    column_prompt = lax.broadcasted_iota(jnp.int32, (1, columns.shape[1]), 1) % prompts
+    zero = jnp.zeros_like(columns)
+    return jnp.concatenate([jnp.where(column_prompt == p, columns, zero) for p in range(prompts)], axis=0)
 
 
 def by_prompt(table, row_prompt, prompts):
@@ -148,9 +155,9 @@
         @pl.loop(0, pos // small)
         def _(s):
             at = pl.multiple_of(j * pos + s * small, small)
-            rows = xb[pl.ds(at, small)].reshape(small * prompts, xb.shape[2])
             to = pl.ds(pl.multiple_of(me * own + at * prompts, small * prompts), small * prompts)
-            nb[to, :] = normed(rows, gain_ref[...]).astype(bf16)
+            nb[to, :] = xb[pl.ds(at, small)].reshape(small * prompts, xb.shape[2])
+            nb[to, :] = normed(nb[to, :], gain_ref[...]).astype(bf16)
 
         if j == 0:
             dec_copy.start()
@@ -163,8 +170,10 @@
         t = product + bias_ref[:, at]
         return (jnp.minimum(t, 0.0) - jnp.log1p(jnp.exp(-jnp.abs(t)))) * (1.0 / decay_tau)
 
+    wide = min(512, own)
+
     def project(at, i):
-        rows = pl.ds(pl.multiple_of(at, chunk), chunk)
+        rows = pl.ds(pl.multiple_of(at, wide), wide)
         kc, vc = slice(i * gk, (i + 1) * gk), slice(i * gv, (i + 1) * gv)
         block = nb[rows, :]
         ks[rows, kc] = dot(block, wk[:, kc]).astype(bf16)
@@ -177,30 +186,36 @@
         kc = slice(i * gk, (i + 1) * gk)
         later[:, kc] = jnp.zeros((8, gk), f32)
 
-        @pl.loop(0, blocks)
+        batch = 4 if blocks % 4 == 0 else 1
+
+        @pl.loop(0, blocks // batch)
         def _(back):
-            at = blocks - 1 - back
-            rows = pl.ds(pl.multiple_of(at * n, n), n)
-            sums = dot(mk_ref[...], halves(gs[rows, kc]))
-            end = ks[rows, kc].astype(f32) * jnp.exp(sums[:n])
-            ek[rows, kc] = end.astype(bf16)
             after = later[:, kc]
-            es[rows, :] = (end * by_prompt(jnp.exp(after), row_prompt, prompts)).astype(bf16)
-            total = sums[n : n + 8]
-            tots[at, :, kc] = total
-            later[:, kc] = after + total
+            for u in range(batch):
+                at = blocks - 1 - back * batch - u
+                rows = pl.ds(pl.multiple_of(at * n, n), n)
+                sums = dot(mk_ref[...], halves(gs[rows, kc]))
+                end = ks[rows, kc].astype(f32) * jnp.exp(sums[:n])
+                ek[rows, kc] = end.astype(bf16)
+                es[rows, :] = (end * by_prompt(jnp.exp(after), row_prompt, prompts)).astype(bf16)
+                total = sums[n : n + 8]
+                tots[at, :, kc] = total
+                after = after + total
+            later[:, kc] = after
 
         span = min(512, rows_all)
         for hh in range(group):
+            st[i * group + hh] = jnp.zeros(st.shape[1:], f32)
+
+        @pl.loop(0, rows_all // span)
+        def _(c):
+            rows = pl.ds(pl.multiple_of(c * span, span), span)
+            for hh in range(group):
+                h = i * group + hh
+                st[h] = st[h] + dot(turned(es[rows, hh * DK : (hh + 1) * DK], prompts), vs[rows, h * DV : (h + 1) * DV])
+
+        for hh in range(group):
             h = i * group + hh
-            hk, hv = slice(hh * DK, (hh + 1) * DK), slice(h * DV, (h + 1) * DV)
-            st[h] = jnp.zeros(st.shape[1:], f32)
-
-            @pl.loop(0, rows_all // span)
-            def _(c):
-                rows = pl.ds(pl.multiple_of(c * span, span), span)
-                st[h] = st[h] + dot_tn(each_prompt(es[rows, hk], prompts), vs[rows, hv])
-
             for p in range(prompts):
                 loc[h * prompts + p] = st[h, p * DK : (p + 1) * DK, :].astype(bf16)
                 tb[i, hh * prompts + p : hh * prompts + p + 1, :] = later[p : p + 1, h * DK : (h + 1) * DK]
@@ -268,28 +283,33 @@
         for s in range(3):
             loads[3 * i + s].wait()
         if i == 0:
-            @pl.loop(0, count)
+            @pl.loop(0, own // wide)
             def _(j):
-                project(me * own + j * chunk, 0)
-
-            @pl.loop(0, count)
+                project(me * own + j * wide, 0)
+
+            @pl.loop(0, own // wide)
             def _(j):
-                piece_copy(j, other).wait_recv()
-                project(other * own + j * chunk, 0)
+                for c in range(wide // chunk):
+                    piece_copy(j * (wide // chunk) + c, other).wait_recv()
+                project(other * own + j * wide, 0)
 
             for h in range(min(2, heads)):
                 state_copy(h).start()
         else:
-            @pl.loop(0, 2 * count)
+            @pl.loop(0, rows_all // wide)
             def _(j):
-                project(j * chunk, i)
+                @pl.when(j == rows_all // wide - 1)
+                def _():
+                    pass_on(i - 1)
+
+                project(j * wide, i)
         keys_of(i)
 
     loads[3 * groups].wait()
 
-    @pl.loop(0, 2 * count)
+    @pl.loop(0, rows_all // wide)
     def _(j):
-        rows = pl.ds(pl.multiple_of(j * chunk, chunk), chunk)
+        rows = pl.ds(pl.multiple_of(j * wide, wide), wide)
         qs[rows, :] = (dot(nb[rows, :], wq[...]) * DK ** (-0.5)).astype(bf16)
 
     for j in range(count):
@@ -299,40 +319,47 @@
     r_at = lax.broadcasted_iota(jnp.int32, (n, n), 0)
     c_at = lax.broadcasted_iota(jnp.int32, (n, n), 1)
 
-    def inside(block):
-        rows = pl.ds(pl.multiple_of(block * n, n), n)
+    def inside(first, several):
         keep = (c_at <= r_at) & (r_at % prompts == c_at % prompts)
-        for i in range(groups):
-            kc = slice(i * gk, (i + 1) * gk)
-            sums = dot(mq_ref[...], halves(gs[rows, kc]))
-            b, d0, d1 = sums[:n], sums[n : n + half], sums[n + half :]
-            q = qs[rows, kc].astype(f32)
-            k = ks[rows, kc].astype(f32)
-            sq[rows, kc] = (q * jnp.exp(b)).astype(bf16)
-            near_q0 = (q[:half] * jnp.exp(d0)).astype(bf16)
-            near_k0 = (k[:half] * jnp.exp(-d0)).astype(bf16)
-            near_q1 = (q[half:] * jnp.exp(d1[half:])).astype(bf16)
-            near_k1 = (k * jnp.exp(-d1)).astype(bf16)
+        rows = [pl.ds(pl.multiple_of((first + u) * n, n), n) for u in range(several)]
+        units = [(rows[u], i) for u in range(several) for i in range(groups)]
+        cols = [slice(i * gk, (i + 1) * gk) for i in range(groups)]
+        sums = [dot(mq_ref[...], halves(gs[at, cols[i]])) for at, i in units]
+        near = []
+        for (at, i), total in zip(units, sums):
+            b, d0, d1 = total[:n], total[n : n + half], total[n + half :]
+            q = qs[at, cols[i]].astype(f32)
+            k = ks[at, cols[i]].astype(f32)
+            sq[at, cols[i]] = (q * jnp.exp(b)).astype(bf16)
+            near.append((
+                (q[:half] * jnp.exp(d0)).astype(bf16),
+                (k[:half] * jnp.exp(-d0)).astype(bf16),
+                (q[half:] * jnp.exp(d1[half:])).astype(bf16),
+                (k * jnp.exp(-d1)).astype(bf16),
+            ))
+        weights = []
+        for (at, i), (q0, k0, q1, k1) in zip(units, near):
             for hh in range(group):
                 hk = slice(hh * DK, (hh + 1) * DK)
-                hv = slice((i * group + hh) * DV, (i * group + hh + 1) * DV)
-                v = vs[rows, hv]
-                w0 = jnp.where(keep[:half, :half], dot_nt(near_q0[:, hk], near_k0[:, hk]), 0.0).astype(bf16)
-                w1 = jnp.where(keep[half:], dot_nt(near_q1[:, hk], near_k1[:, hk]), 0.0).astype(bf16)
-                oi[rows, hv] = jnp.concatenate([dot(w0, v[:half]), dot(w1, v)], axis=0).astype(bf16)
-
-    pass_on(0)
-
-    @pl.loop(0, blocks // 2)
-    def _(block):
-        inside(block)
-
-    for i in range(1, groups):
-        pass_on(i)
-
-    @pl.loop(blocks // 2, blocks)
-    def _(block):
-        inside(block)
+                weights.append((at, i * group + hh, dot_nt(q0[:, hk], k0[:, hk]), dot_nt(q1[:, hk], k1[:, hk])))
+        for at, h, w0, w1 in weights:
+            hv = slice(h * DV, (h + 1) * DV)
+            v = vs[at, hv]
+            w0 = jnp.where(keep[:half, :half], w0, 0.0).astype(bf16)
+            w1 = jnp.where(keep[half:], w1, 0.0).astype(bf16)
+            oi[at, hv] = jnp.concatenate([dot(w0, v[:half]), dot(w1, v)], axis=0).astype(bf16)
+
+    pairs = blocks // 2
+
+    @pl.loop(0, pairs // 2)
+    def _(pair):
+        inside(2 * pair, 2)
+
+    pass_on(groups - 1)
+
+    @pl.loop(pairs // 2, pairs)
+    def _(pair):
+        inside(2 * pair, 2)
 
     def head_norm(block, h):
         factor = lax.rsqrt(jnp.mean(block * block, axis=-1, keepdims=True) + norm_eps)
@@ -347,8 +374,8 @@
     for h in range(heads):
         at = slice(h * DK, (h + 1) * DK)
         qet[h] = jnp.transpose(q_d[:, at] * e_d[:, at])
-        cols_ref[0, h] = jnp.transpose(e_d[:, at])
-        cols_ref[1, h] = jnp.transpose(k_d[:, at])
+    for s, table in enumerate((e_d, k_d)):
+        cols_ref[s] = jnp.transpose(jnp.concatenate([table[:, h * DK : (h + 1) * DK] for h in range(heads)], axis=0))
     attb[...] = jnp.zeros_like(attb)
     for h in range(heads):
         state_copy(h).wait()
@@ -372,54 +399,51 @@
     )
     dec_give.start()
 
-    def out_refs(side, j, i):
+    def out_refs(side, j):
         rows = pl.ds(pl.multiple_of(side * own + j * n, n), n)
-        cols = pl.ds(pl.multiple_of(me * vw + i * gv, gv), gv)
-        return oi.at[rows, pl.ds(i * gv, gv)], nrm_hbm.at[pl.ds(pl.multiple_of(j * n, n), n), cols]
-
-    def keep_copy(j, i):
-        src, dst = out_refs(me, j, i)
-        return pltpu.make_async_copy(src, dst, out_local.at[i, j])
-
-    def give_copy(j, i):
-        src, dst = out_refs(other, j, i)
+        return oi.at[rows], nrm_hbm.at[pl.ds(pl.multiple_of(j * n, n), n), my_cols]
+
+    def keep_copy(j):
+        src, dst = out_refs(me, j)
+        return pltpu.make_async_copy(src, dst, out_local.at[j])
+
+    def give_copy(j):
+        src, dst = out_refs(other, j)
         return pltpu.make_async_remote_copy(
-            src_ref=src, dst_ref=dst, send_sem=out_send.at[i, j], recv_sem=out_recv.at[i, j],
+            src_ref=src, dst_ref=dst, send_sem=out_send.at[j], recv_sem=out_recv.at[j],
             device_id={"tp": other}, device_id_type=MESH,
         )
 
     for i in range(groups):
         for d in range(1, kv):
             incoming_copy(d, i).wait_recv()
-        for hh in range(group):
-            h = i * group + hh
+    for h in range(heads):
+        for p in range(prompts):
+            st[h, p * DK : (p + 1) * DK, :] = sin[h * prompts + p].astype(f32)
+
+    @pl.loop(0, blocks)
+    def _(block):
+        rows = pl.ds(pl.multiple_of(block * n, n), n)
+        for h in range(heads):
+            hk, hv = slice(h * DK, (h + 1) * DK), slice(h * DV, (h + 1) * DV)
+            state = st[h]
+            from_state = dot(each_prompt(sq[rows, hk], prompts), state.astype(bf16))
+            oi[rows, hv] = head_norm(oi[rows, hv].astype(f32) + from_state, h)
+            added = dot(turned(ek[rows, hk], prompts), vs[rows, hv])
+            decay = jnp.transpose(jnp.exp(tots[block, :, hk]))
             for p in range(prompts):
-                st[h, p * DK : (p + 1) * DK, :] = sin[h * prompts + p].astype(f32)
-
-        @pl.loop(0, blocks)
-        def _(block):
-            rows = pl.ds(pl.multiple_of(block * n, n), n)
-            for hh in range(group):
-                h = i * group + hh
-                hk, hv = slice(h * DK, (h + 1) * DK), slice(h * DV, (h + 1) * DV)
-                state = st[h]
-                from_state = dot(each_prompt(sq[rows, hk], prompts), state.astype(bf16))
-                oi[rows, hv] = head_norm(oi[rows, hv].astype(f32) + from_state, h)
-                added = dot_tn(each_prompt(ek[rows, hk], prompts), vs[rows, hv])
-                decay = jnp.transpose(jnp.exp(tots[block, :, hk]))
-                for p in range(prompts):
-                    at = slice(p * DK, (p + 1) * DK)
-                    st[h, at, :] = state[at] * decay[:, p : p + 1] + added[at]
-            side = block // (blocks // 2)
-            j = block - side * (blocks // 2)
-
-            @pl.when(side == me)
-            def _():
-                keep_copy(j, i).start()
-
-            @pl.when(side != me)
-            def _():
-                give_copy(j, i).start()
+                at = slice(p * DK, (p + 1) * DK)
+                st[h, at, :] = state[at] * decay[:, p : p + 1] + added[at]
+        side = block // (blocks // 2)
+        j = block - side * (blocks // 2)
+
+        @pl.when(side == me)
+        def _():
+            keep_copy(j).start()
+
+        @pl.when(side != me)
+        def _():
+            give_copy(j).start()
 
     for d in range(1, kv):
         for h in range(heads):
@@ -429,20 +453,20 @@
             incoming_copy(d, i).wait_send()
     dec_keep.wait()
     dec_give.wait()
-    for i in range(groups):
-        @pl.loop(0, blocks // 2)
-        def _(j):
-            keep_copy(j, i).wait()
-            give_copy(j, i).wait_send()
-            give_copy(j, i).wait_recv()
+
+    @pl.loop(0, blocks // 2)
+    def _(j):
+        keep_copy(j).wait()
+        give_copy(j).wait_send()
+        give_copy(j).wait_recv()
 
 
 def last_kernel(
     own_pos, prompts, heads, dec_own,
-    nrm_hbm, ndec_ref, w_hbm, ds_hbm, cols_ref, vrow_ref, ps_ref,
-    y_hbm, yd_ref, po_ref, do_hbm,
-    nrm, w, yb, sb,
-    n_sem, w_sem, s_sem, y_sem, o_sem,
+    nrm_hbm, ndec_hbm, w_hbm, ds_hbm, cols_hbm, vrow_hbm, ps_hbm,
+    y_hbm, yd_hbm, po_hbm, do_hbm,
+    nrm, w, yb, sb, yd, cols, vrow, ps,
+    n_sem, w_sem, s_sem, y_sem, o_sem, a_sem,
 ):
     own = own_pos * prompts
     chunk = min(256, own)
@@ -470,35 +494,64 @@
         at = pl.ds(t * tile, tile)
         return pltpu.make_async_copy(yb.at[:, :, at], y_hbm.at[:, :, at], y_sem.at[t])
 
+    first = w_hbm.shape[0] // 2
+    w_first = [
+        pltpu.make_async_copy(w_hbm.at[pl.ds(c * first, first), pl.ds(0, tile)], w.at[pl.ds(c * first, first), pl.ds(0, tile)], a_sem.at[c])
+        for c in range(2)
+    ]
+    small = [
+        pltpu.make_async_copy(src, dst, a_sem.at[2 + c])
+        for c, (src, dst) in enumerate(((ndec_hbm, nrm.at[pl.ds(own, PAD)]), (cols_hbm, cols), (vrow_hbm, vrow), (ps_hbm, ps)))
+    ]
     n_copy(0).start()
-    w_copy(0).start()
+    for load in w_first + small:
+        load.start()
     for j in range(1, count):
         n_copy(j).start()
     s_copy(0).start()
-    for t in range(1, heads):
-        w_copy(t).start()
-        s_copy(t).start()
-    po_ref[...] = ps_ref[...]
+    ps_out = pltpu.make_async_copy(ps, po_hbm, a_sem.at[6])
+    yd_out = pltpu.make_async_copy(yd, yd_hbm, a_sem.at[7])
+    each = -(-seqs // count)
     for t in range(heads):
         at = slice(t * tile, (t + 1) * tile)
-        w_copy(t).wait()
-        s_copy(t).wait()
-        each = -(-seqs // count)
+        if t == 0:
+            n_copy(0).wait()
+            for load in w_first:
+                load.wait()
+        else:
+            w_copy(t).wait()
+        if t + 1 < heads:
+            w_copy(t + 1).start()
+            s_copy(t + 1).start()
         for j in range(count):
-            if t == 0:
+            if t == 0 and j:
                 n_copy(j).wait()
-            block = dot(nrm[j * chunk : (j + 1) * chunk, :], w[:, at]).astype(bf16)
-            yb[j * pos : (j + 1) * pos, :, at] = block.reshape(pos, prompts, tile)
+            if t == 0 and j == count - 1:
+                small[0].wait()
+            extra = PAD if j == count - 1 else 0
+            block = dot(nrm[j * chunk : (j + 1) * chunk + extra, :], w[:, at])
+            yb[j * pos : (j + 1) * pos, :, at] = block[:chunk].astype(bf16).reshape(pos, prompts, tile)
+            if extra:
+                yd[:, at] = block[chunk : chunk + dec_own].astype(bf16)
+            if j == 0:
+                s_copy(t).wait()
+            if t == 0 and j == 0:
+                for load in small[1:]:
+                    load.wait()
+                ps_out.start()
             for s in range(j * each, min(seqs, (j + 1) * each)):
                 row = (s // dec_own) * PAD + s % dec_own
-                v = vrow_ref[row : row + 1, t * DV : (t + 1) * DV]
-                sb[t, s] = sb[t, s] * cols_ref[0, t, :, row : row + 1] + cols_ref[1, t, :, row : row + 1] * v
-        yd_ref[:, at] = dot(ndec_ref[...], w[:, at])[:dec_own].astype(bf16)
+                v = vrow[row : row + 1, t * DV : (t + 1) * DV]
+                at_row = slice(t * 2 * PAD + row, t * 2 * PAD + row + 1)
+                sb[t, s] = sb[t, s] * cols[0, :, at_row] + cols[1, :, at_row] * v
         y_copy(t).start()
         o_copy(t).start()
+    yd_out.start()
     for t in range(heads):
         y_copy(t).wait()
         o_copy(t).wait()
+    ps_out.wait()
+    yd_out.wait()
 
 
 ANY = pl.BlockSpec(memory_space=pl.ANY)
@@ -534,7 +587,7 @@
             jax.ShapeDtypeStruct((own, 2 * vw), bf16),
             jax.ShapeDtypeStruct((PAD, 2 * vw), bf16),
             jax.ShapeDtypeStruct(prompt_state.shape, f32),
-            jax.ShapeDtypeStruct((2, heads, DK, 2 * PAD), f32),
+            jax.ShapeDtypeStruct((2, DK, heads * 2 * PAD), f32),
             jax.ShapeDtypeStruct((2 * PAD, vw), f32),
         ),
         in_specs=[ANY, VMEM, ANY, ANY, ANY, ANY, VMEM, VMEM, VMEM, VMEM, VMEM, VMEM, ANY],
@@ -582,9 +635,9 @@
             dma((kv, groups)),
             dma((kv, groups)),
             dma((heads,)),
-            dma((groups, blocks // 2)),
-            dma((groups, blocks // 2)),
-            dma((groups, blocks // 2)),
+            dma((blocks // 2,)),
+            dma((blocks // 2,)),
+            dma((blocks // 2,)),
             dma,
             dma,
             dma,
@@ -603,18 +656,23 @@
             jax.ShapeDtypeStruct(prompt_state.shape, f32),
             jax.ShapeDtypeStruct(decode_state.shape, f32),
         ),
-        in_specs=[ANY, VMEM, ANY, ANY, VMEM, VMEM, VMEM],
-        out_specs=(ANY, VMEM, VMEM, ANY),
+        in_specs=[ANY] * 7,
+        out_specs=(ANY,) * 4,
         scratch_shapes=[
-            pltpu.VMEM((own, 2 * vw), bf16),
+            pltpu.VMEM((own + PAD, 2 * vw), bf16),
             pltpu.VMEM(w_out.shape, bf16),
             pltpu.VMEM(pieces.shape, bf16),
             pltpu.VMEM((heads, seqs, DK, DV), f32),
+            pltpu.VMEM(new_tokens.shape, bf16),
+            pltpu.VMEM(cols.shape, f32),
+            pltpu.VMEM(v_rows.shape, f32),
+            pltpu.VMEM(prompt_state.shape, f32),
             dma((count,)),
             dma((heads,)),
             dma((heads,)),
             dma((heads,)),
             dma((heads,)),
+            dma((8,)),
         ],
         compiler_params=pltpu.CompilerParams(vmem_limit_bytes=LIMIT),
     )(nrm, ndec, w_out, decode_state, cols, v_rows, prompt_out)

time: 109 us -> 85 us (0.78)
  Pallas kernels: 108 us -> 84 us
    pallas_call x1, Pallas kernels: 89.7 us -> 68.1 us  [on_device(): pl.pallas_call(functools.partial(main_kernel, own_pos, prompts, heads, kv...]
    pallas_call x1, Pallas kernels: 18.2 us -> 15.9 us  [on_device(): pl.pallas_call(functools.partial(last_kernel, own_pos, prompts, heads, de...]
where the time goes in v2:
time: 85 us; the launch traced here: 84.8 us
  Pallas kernels  84 us (99%)
    pallas_call x1, Pallas kernels, on_device(): pl.pallas_call(functools.partial(main_kernel, own_pos, prompts, heads, kv...  68.1 us
    pallas_call x1, Pallas kernels, on_device(): pl.pallas_call(functools.partial(last_kernel, own_pos, prompts, heads, de...  15.9 us

profile of v2, /device:TPU:0, one launch (start us, length us, event | category | flops | bytes accessed | tf_op | source)
XLA Modules:
  0.0 84.8 jit_solution(6703593912052734569)
XLA Ops:
  0.6 68.1 %layer.1 = (bf16[1024,2048]{1,0:T(8,128)(2,1)}, bf16[16,2048]{1,0:T(8,128)(2,1)}, f32[2,4,32,256]{3,2,1,0:T(8,128)}, f32[2,128,128]{2,1,0:T(8,128)}, f32[32,1024]{1,0:T(8,128)}) custom-call(bf16[512,2,2048]{2,1,0:T(2,128)(2,1)} %x_hbm.1, bf16[8,2048]{1,0:T(8,128)(2,1)} %dec_ref.1, bf16[2048,512]{1,0:T(8,128)(2,1)} %wq_hbm.1, bf16[2048,512]{1,0:T(8,128)(2,1)} %wk_hbm.1, ...), custom_call_target="tpu_custom_call" | custom-call | tf_op jit(solution)/shard_map/layer/pallas_call | solution.py:583
  68.7 15.9 %last.1 = (bf16[512,2,2048]{2,1,0:T(2,128)(2,1)}, bf16[8,2048]{1,0:T(8,128)(2,1)}, f32[2,4,32,256]{3,2,1,0:T(8,128)}, f32[16,4,128,256]{3,2,1,0:T(8,128)}) custom-call(bf16[1024,2048]{1,0:T(8,128)(2,1)} %get-tuple-element.9.nrm_hbm, bf16[16,2048]{1,0:T(8,128)(2,1)} %get-tuple-element.10.ndec_hbm, bf16[2048,2048]{1,0:T(8,128)(2,1)} %w_hbm.1, ...), custom_call_target="tpu_custom_call" | custom-call | tf_op jit(solution)/shard_map/last/pallas_call | solution.py:650

commit v3 on v2

--- a/solution.py
+++ b/solution.py
@@ -84,10 +84,10 @@
 
 def main_kernel(
     own_pos, prompts, heads, kv, dec_own,
-    x_hbm, dec_ref, wq_hbm, wk_hbm, wv_hbm, wd_hbm, bias_ref, gain_ref, head_gain_ref, mk_ref, mq_ref, ps_ref, ds_hbm,
+    x_hbm, dec_ref, wq_hbm, wk_hbm, wv_hbm, wd_hbm, bias_ref, gain_ref, head_gain_ref, mk_hbm, mq_hbm, ps_hbm, ds_hbm,
     nrm_hbm, ndec_hbm, po_ref, cols_ref, vrow_ref,
-    xb, nb, nd, wq, wk, wv, wd, qs, ks, vs, gs, sq, ek, es, oi, tots, later, st, loc, rx, inc, sin, tb, rxt, ttr,
-    sbuf, qet, attb, dl,
+    xb, nb, nd, wq, wkd, wv, mk_ref, mq_ref, ps_ref, qs, ks, vs, gs, sq, ek, ew, oi, tots, later, st, loc, rx, inc, sin, tb, rxt, ttr,
+    sbuf, qet, attb, scores, dl,
     x_sem, w_sem, n_send, n_recv, nd_send, nd_recv, p1_send, p1_recv, t_send, t_recv, p2_send, p2_recv,
     s_sem, out_local, out_send, out_recv, d_local, d_send, d_recv,
 ):
@@ -104,6 +104,7 @@
     group = 2 if heads % 2 == 0 else 1
     groups = heads // group
     gk, gv = group * DK, group * DV
+    near_group = 2 if heads % 2 == 0 else 1
     qk, vw = heads * DK, heads * DV
     part = DK // kv
     seqs = 2 * dec_own
@@ -118,9 +119,14 @@
     loads = []
     for i in range(groups):
         kc, vc = pl.ds(i * gk, gk), pl.ds(i * gv, gv)
-        for s, (src, dst, cols) in enumerate(((wk_hbm, wk, kc), (wd_hbm, wd, kc), (wv_hbm, wv, vc))):
-            loads.append(pltpu.make_async_copy(src.at[:, cols], dst.at[:, cols], w_sem.at[3 * i + s]))
-    loads.append(pltpu.make_async_copy(wq_hbm, wq, w_sem.at[3 * groups]))
+        for s, (src, dst) in enumerate((
+            (wk_hbm.at[:, kc], wkd.at[:, pl.ds(2 * i * gk, gk)]),
+            (wd_hbm.at[:, kc], wkd.at[:, pl.ds((2 * i + 1) * gk, gk)]),
+            (wv_hbm.at[:, vc], wv.at[:, vc]),
+        )):
+            loads.append(pltpu.make_async_copy(src, dst, w_sem.at[3 * i + s]))
+    for s, (src, dst) in enumerate(((wq_hbm, wq), (mk_hbm, mk_ref), (mq_hbm, mq_ref), (ps_hbm, ps_ref))):
+        loads.append(pltpu.make_async_copy(src, dst, w_sem.at[3 * groups + s]))
     for load in loads:
         load.start()
 
@@ -131,7 +137,7 @@
     pl.semaphore_wait(barrier, kv)
 
     def state_copy(h):
-        return pltpu.make_async_copy(ds_hbm.at[:, h], sbuf.at[h % 2], s_sem.at[h])
+        return pltpu.make_async_copy(ds_hbm.at[:, h], sbuf.at[lax.rem(h, 2)], s_sem.at[h])
 
     def piece_copy(j, side):
         rows = pl.ds(pl.multiple_of(side * own + j * chunk, chunk), chunk)
@@ -176,31 +182,44 @@
         rows = pl.ds(pl.multiple_of(at, wide), wide)
         kc, vc = slice(i * gk, (i + 1) * gk), slice(i * gv, (i + 1) * gv)
         block = nb[rows, :]
-        ks[rows, kc] = dot(block, wk[:, kc]).astype(bf16)
+        pair = dot(block, wkd[:, 2 * i * gk : 2 * (i + 1) * gk])
+        ks[rows, kc] = pair[:, :gk].astype(bf16)
+        gs[rows, kc] = decay_of(pair[:, gk:], i)
         vs[rows, vc] = dot(block, wv[:, vc]).astype(bf16)
-        gs[rows, kc] = decay_of(dot(block, wd[:, kc]), i)
 
     row_prompt = lax.broadcasted_iota(jnp.int32, (n, 1), 0) % prompts
+
+    def at_odd(u):
+        return u % 2 == 0
 
     def keys_of(i):
         kc = slice(i * gk, (i + 1) * gk)
         later[:, kc] = jnp.zeros((8, gk), f32)
 
-        batch = 4 if blocks % 4 == 0 else 1
+        batch = 4 if blocks % 4 == 0 else 2
 
         @pl.loop(0, blocks // batch)
         def _(back):
             after = later[:, kc]
+            places = [blocks - 1 - back * batch - u for u in range(batch)]
+            spans = [pl.ds(pl.multiple_of(at * n, n), n) for at in places]
+            together = [
+                dot(mk_ref[...], jnp.concatenate([halves(gs[spans[u], kc]), halves(gs[spans[u + 1], kc])], axis=1))
+                for u in range(0, batch, 2)
+            ]
             for u in range(batch):
-                at = blocks - 1 - back * batch - u
-                rows = pl.ds(pl.multiple_of(at * n, n), n)
-                sums = dot(mk_ref[...], halves(gs[rows, kc]))
+                at, rows = places[u], spans[u]
+                sums = together[u // 2][:, (u % 2) * gk : (u % 2 + 1) * gk]
                 end = ks[rows, kc].astype(f32) * jnp.exp(sums[:n])
-                ek[rows, kc] = end.astype(bf16)
-                es[rows, :] = (end * by_prompt(jnp.exp(after), row_prompt, prompts)).astype(bf16)
+                if at_odd(u):
+                    ek[rows, kc] = end.astype(bf16)
+                else:
+                    ek[rows, kc] = (end * by_prompt(jnp.exp(following), row_prompt, prompts)).astype(bf16)
+                    ew[pl.ds(pl.multiple_of((at // 2) * n, n), n), kc] = end.astype(bf16)
+                sq[rows, :gk] = (end * by_prompt(jnp.exp(after), row_prompt, prompts)).astype(bf16)
                 total = sums[n : n + 8]
                 tots[at, :, kc] = total
-                after = after + total
+                after, following = after + total, total
             later[:, kc] = after
 
         span = min(512, rows_all)
@@ -212,7 +231,7 @@
             rows = pl.ds(pl.multiple_of(c * span, span), span)
             for hh in range(group):
                 h = i * group + hh
-                st[h] = st[h] + dot(turned(es[rows, hh * DK : (hh + 1) * DK], prompts), vs[rows, h * DV : (h + 1) * DV])
+                st[h] = st[h] + dot(turned(sq[rows, hh * DK : (hh + 1) * DK], prompts), vs[rows, h * DV : (h + 1) * DV])
 
         for hh in range(group):
             h = i * group + hh
@@ -238,46 +257,40 @@
             device_id={"kv": lax.rem(here + d, kv)}, device_id_type=MESH,
         )
 
-    def incoming_copy(d, i):
+    def incoming_copy(d, h):
         to = lax.rem(here + d, kv)
-        hp = pl.ds(i * group * prompts, group * prompts)
+        hp = pl.ds(h * prompts, prompts)
         return pltpu.make_async_remote_copy(
             src_ref=inc.at[to, hp], dst_ref=sin.at[hp, pl.ds(pl.multiple_of(here * part, part), part)],
-            send_sem=p2_send.at[d, i], recv_sem=p2_recv.at[d, i], device_id={"kv": to}, device_id_type=MESH,
+            send_sem=p2_send.at[d, h], recv_sem=p2_recv.at[d, h], device_id={"kv": to}, device_id_type=MESH,
         )
 
     my_part = pl.ds(pl.multiple_of(here * part, part), part)
 
-    def pass_on(i):
+    def pass_on(h):
+        i, hh = h // group, h % group
         for d in range(1, kv):
-            total_copy(d, i).wait_recv()
-            for hh in range(group):
-                local_copy(d, i * group + hh).wait_recv()
-        rxt[0, i] = tb[i]
-        for hh in range(group):
-            for p in range(prompts):
-                hp = (i * group + hh) * prompts + p
-                rx[0, hp] = loc[hp, my_part, :]
-        for c in range(kv):
-            d = lax.rem(here - c + kv, kv)
-            ttr[c] = jnp.transpose(jnp.exp(rxt[d, i]))
-        for hh in range(group):
-            h = i * group + hh
-            for p in range(prompts):
-                hp = h * prompts + p
-                running = ps_ref[p, h]
-                for c in range(kv):
-                    d = lax.rem(here - c + kv, kv)
-                    inc[c, hp] = running.astype(bf16)
-                    at = hh * prompts + p
-                    running = running * ttr[c, my_part, at : at + 1] + rx[d, hp].astype(f32)
-                po_ref[p, h] = running
+            if hh == 0:
+                total_copy(d, i).wait_recv()
+            local_copy(d, h).wait_recv()
+        if hh == 0:
+            rxt[0, i] = tb[i]
+            for c in range(kv):
+                ttr[c] = jnp.transpose(jnp.exp(rxt[lax.rem(here - c + kv, kv), i]))
+        for p in range(prompts):
+            hp = h * prompts + p
+            rx[0, hp] = loc[hp, my_part, :]
+            running = ps_ref[p, h]
+            at = hh * prompts + p
+            for c in range(kv):
+                inc[c, hp] = running.astype(bf16)
+                running = running * ttr[c, my_part, at : at + 1] + rx[lax.rem(here - c + kv, kv), hp].astype(f32)
+            po_ref[p, h] = running
         for d in range(1, kv):
-            incoming_copy(d, i).start()
-        for hh in range(group):
-            for p in range(prompts):
-                hp = (i * group + hh) * prompts + p
-                sin[hp, my_part, :] = inc[here, hp]
+            incoming_copy(d, h).start()
+        for p in range(prompts):
+            hp = h * prompts + p
+            sin[hp, my_part, :] = inc[here, hp]
 
     for i in range(groups):
         for s in range(3):
@@ -295,71 +308,22 @@
 
             for h in range(min(2, heads)):
                 state_copy(h).start()
+            for load in loads[3 * groups :]:
+                load.wait()
         else:
             @pl.loop(0, rows_all // wide)
             def _(j):
-                @pl.when(j == rows_all // wide - 1)
-                def _():
-                    pass_on(i - 1)
-
                 project(j * wide, i)
+
+        if i:
+            for hh in range(group):
+                pass_on((i - 1) * group + hh)
         keys_of(i)
 
-    loads[3 * groups].wait()
-
-    @pl.loop(0, rows_all // wide)
-    def _(j):
-        rows = pl.ds(pl.multiple_of(j * wide, wide), wide)
-        qs[rows, :] = (dot(nb[rows, :], wq[...]) * DK ** (-0.5)).astype(bf16)
 
     for j in range(count):
         piece_copy(j, me).wait_send()
     dec_copy.wait()
-
-    r_at = lax.broadcasted_iota(jnp.int32, (n, n), 0)
-    c_at = lax.broadcasted_iota(jnp.int32, (n, n), 1)
-
-    def inside(first, several):
-        keep = (c_at <= r_at) & (r_at % prompts == c_at % prompts)
-        rows = [pl.ds(pl.multiple_of((first + u) * n, n), n) for u in range(several)]
-        units = [(rows[u], i) for u in range(several) for i in range(groups)]
-        cols = [slice(i * gk, (i + 1) * gk) for i in range(groups)]
-        sums = [dot(mq_ref[...], halves(gs[at, cols[i]])) for at, i in units]
-        near = []
-        for (at, i), total in zip(units, sums):
-            b, d0, d1 = total[:n], total[n : n + half], total[n + half :]
-            q = qs[at, cols[i]].astype(f32)
-            k = ks[at, cols[i]].astype(f32)
-            sq[at, cols[i]] = (q * jnp.exp(b)).astype(bf16)
-            near.append((
-                (q[:half] * jnp.exp(d0)).astype(bf16),
-                (k[:half] * jnp.exp(-d0)).astype(bf16),
-                (q[half:] * jnp.exp(d1[half:])).astype(bf16),
-                (k * jnp.exp(-d1)).astype(bf16),
-            ))
-        weights = []
-        for (at, i), (q0, k0, q1, k1) in zip(units, near):
-            for hh in range(group):
-                hk = slice(hh * DK, (hh + 1) * DK)
-                weights.append((at, i * group + hh, dot_nt(q0[:, hk], k0[:, hk]), dot_nt(q1[:, hk], k1[:, hk])))
-        for at, h, w0, w1 in weights:
-            hv = slice(h * DV, (h + 1) * DV)
-            v = vs[at, hv]
-            w0 = jnp.where(keep[:half, :half], w0, 0.0).astype(bf16)
-            w1 = jnp.where(keep[half:], w1, 0.0).astype(bf16)
-            oi[at, hv] = jnp.concatenate([dot(w0, v[:half]), dot(w1, v)], axis=0).astype(bf16)
-
-    pairs = blocks // 2
-
-    @pl.loop(0, pairs // 2)
-    def _(pair):
-        inside(2 * pair, 2)
-
-    pass_on(groups - 1)
-
-    @pl.loop(pairs // 2, pairs)
-    def _(pair):
-        inside(2 * pair, 2)
 
     def head_norm(block, h):
         factor = lax.rsqrt(jnp.mean(block * block, axis=-1, keepdims=True) + norm_eps)
@@ -368,28 +332,49 @@
 
     new = nd[...]
     q_d = (dot(new, wq[...]) * DK ** (-0.5)).astype(bf16).astype(f32)
-    k_d = dot(new, wk[...]).astype(bf16).astype(f32)
-    e_d = jnp.exp(decay_of(dot(new, wd[...]), 0))
+    pair_d = dot(new, wkd[...])
+    k_d = jnp.concatenate([pair_d[:, 2 * i * gk : (2 * i + 1) * gk] for i in range(groups)], axis=1).astype(bf16).astype(f32)
+    e_d = jnp.exp(jnp.concatenate([decay_of(pair_d[:, (2 * i + 1) * gk : 2 * (i + 1) * gk], i) for i in range(groups)], axis=1))
     vrow_ref[...] = dot(new, wv[...]).astype(bf16).astype(f32)
     for h in range(heads):
         at = slice(h * DK, (h + 1) * DK)
         qet[h] = jnp.transpose(q_d[:, at] * e_d[:, at])
+        score = jnp.sum(q_d[:, at] * k_d[:, at], axis=-1, keepdims=True)
+        scores[:, h * DV : (h + 1) * DV] = score * vrow_ref[:, h * DV : (h + 1) * DV]
     for s, table in enumerate((e_d, k_d)):
         cols_ref[s] = jnp.transpose(jnp.concatenate([table[:, h * DK : (h + 1) * DK] for h in range(heads)], axis=0))
     attb[...] = jnp.zeros_like(attb)
-    for h in range(heads):
-        state_copy(h).wait()
+
+    def queries(j):
+        rows = pl.ds(pl.multiple_of(j * wide, wide), wide)
+        qs[rows, :] = (dot(nb[rows, :], wq[...]) * DK ** (-0.5)).astype(bf16)
+
+    def attend(h):
+        slot = lax.rem(h, 2)
+        hv = pl.ds(pl.multiple_of(h * DV, DV), DV)
         for s in range(seqs):
             row = (s // dec_own) * PAD + s % dec_own
-            attb[row : row + 1, h * DV : (h + 1) * DV] = jnp.sum(
-                sbuf[h % 2, s] * qet[h, :, row : row + 1], axis=0, keepdims=True
-            )
-        if h + 2 < heads:
+            attb[row : row + 1, hv] = jnp.sum(sbuf[slot, s] * qet[h, :, row : row + 1], axis=0, keepdims=True)
+
+    @pl.loop(0, heads)
+    def _(h):
+        state_copy(h).wait()
+        if rows_all // wide == heads:
+            queries(h)
+        attend(h)
+
+        @pl.when(h + 2 < heads)
+        def _():
             state_copy(h + 2).start()
+
+    if rows_all // wide != heads:
+        @pl.loop(0, rows_all // wide)
+        def _(j):
+            queries(j)
+
     for h in range(heads):
-        at, hv = slice(h * DK, (h + 1) * DK), slice(h * DV, (h + 1) * DV)
-        score = jnp.sum(q_d[:, at] * k_d[:, at], axis=-1, keepdims=True)
-        dl[:, hv] = head_norm(attb[:, hv] + score * vrow_ref[:, hv], h)
+        hv = slice(h * DV, (h + 1) * DV)
+        dl[:, hv] = head_norm(attb[:, hv] + scores[:, hv], h)
     my_cols = pl.ds(pl.multiple_of(me * vw, vw), vw)
     dec_keep = pltpu.make_async_copy(dl.at[mine], ndec_hbm.at[:, my_cols], d_local)
     dec_keep.start()
@@ -399,66 +384,134 @@
     )
     dec_give.start()
 
-    def out_refs(side, j):
-        rows = pl.ds(pl.multiple_of(side * own + j * n, n), n)
-        return oi.at[rows], nrm_hbm.at[pl.ds(pl.multiple_of(j * n, n), n), my_cols]
-
-    def keep_copy(j):
-        src, dst = out_refs(me, j)
-        return pltpu.make_async_copy(src, dst, out_local.at[j])
-
-    def give_copy(j):
-        src, dst = out_refs(other, j)
+    r_at = lax.broadcasted_iota(jnp.int32, (n, n), 0)
+    c_at = lax.broadcasted_iota(jnp.int32, (n, n), 1)
+
+    def inside(pair):
+        same = r_at % prompts == c_at % prompts
+        keep = (c_at <= r_at) & same
+        both = pl.ds(pl.multiple_of(pair * 2 * n, 2 * n), 2 * n)
+        rows = [pl.ds(pl.multiple_of((2 * pair + u) * n, n), n) for u in range(2)]
+        early = pl.ds(pl.multiple_of(pair * n, n), n)
+        units = [(u, i) for u in range(2) for i in range(heads // near_group)]
+        cols = [slice(i * near_group * DK, (i + 1) * near_group * DK) for i in range(heads // near_group)]
+        sums = [dot(mq_ref[...], halves(gs[rows[u], cols[i]])) for u, i in units]
+        near = []
+        for (u, i), total in zip(units, sums):
+            b, d0, d1 = total[:n], total[n : n + half], total[n + half :]
+            q = qs[rows[u], cols[i]].astype(f32)
+            k = ks[rows[u], cols[i]].astype(f32)
+            start = q * jnp.exp(b)
+            across = None
+            if u:
+                across = start.astype(bf16)
+                start = start * by_prompt(jnp.exp(tots[2 * pair, :, cols[i]]), row_prompt, prompts)
+            sq[rows[u], cols[i]] = start.astype(bf16)
+            near.append((
+                (q[:half] * jnp.exp(d0)).astype(bf16),
+                (k[:half] * jnp.exp(-d0)).astype(bf16),
+                (q[half:] * jnp.exp(d1[half:])).astype(bf16),
+                (k * jnp.exp(-d1)).astype(bf16),
+                across,
+            ))
+        weights = []
+        for (u, i), (q0, k0, q1, k1, across) in zip(units, near):
+            for hh in range(near_group):
+                h = i * near_group + hh
+                hk = slice(hh * DK, (hh + 1) * DK)
+                w2 = dot_nt(across[:, hk], ew[early, h * DK : (h + 1) * DK]) if u else None
+                weights.append((u, h, dot_nt(q0[:, hk], k0[:, hk]), dot_nt(q1[:, hk], k1[:, hk]), w2))
+        for u, h, w0, w1, w2 in weights:
+            hv = slice(h * DV, (h + 1) * DV)
+            w0 = jnp.where(keep[:half, :half], w0, 0.0).astype(bf16)
+            w1 = jnp.where(keep[half:], w1, 0.0).astype(bf16)
+            v = vs[rows[0], hv]
+            if u:
+                v = vs[both, hv]
+                w2 = jnp.where(same, w2, 0.0).astype(bf16)
+                w0 = jnp.concatenate([w2[:half], w0], axis=1)
+                w1 = jnp.concatenate([w2[half:], w1], axis=1)
+            oi[rows[u], hv] = jnp.concatenate([dot(w0, v[: w0.shape[1]]), dot(w1, v)], axis=0).astype(bf16)
+
+    pairs = blocks // 2
+
+    due = [2 * pairs // 4 if hh == 0 else 3 * pairs // 4 for hh in range(group)]
+    marks = sorted(set([0, pairs] + due))
+    for low, high in zip(marks[:-1], marks[1:]):
+        @pl.loop(low, high)
+        def _(pair):
+            inside(pair)
+
+        for hh in range(group):
+            if due[hh] == high:
+                pass_on((groups - 1) * group + hh)
+
+    def out_refs(side, j, i):
+        rows = pl.ds(pl.multiple_of(side * own + j * 2 * n, 2 * n), 2 * n)
+        to = pl.ds(pl.multiple_of(me * vw + i * gv, gv), gv)
+        return oi.at[rows, pl.ds(i * gv, gv)], nrm_hbm.at[pl.ds(pl.multiple_of(j * 2 * n, 2 * n), 2 * n), to]
+
+    def keep_copy(j, i):
+        src, dst = out_refs(me, j, i)
+        return pltpu.make_async_copy(src, dst, out_local.at[i, j])
+
+    def give_copy(j, i):
+        src, dst = out_refs(other, j, i)
         return pltpu.make_async_remote_copy(
-            src_ref=src, dst_ref=dst, send_sem=out_send.at[j], recv_sem=out_recv.at[j],
+            src_ref=src, dst_ref=dst, send_sem=out_send.at[i, j], recv_sem=out_recv.at[i, j],
             device_id={"tp": other}, device_id_type=MESH,
         )
 
+    def scan(i):
+        members = range(i * group, (i + 1) * group)
+        for h in members:
+            for d in range(1, kv):
+                incoming_copy(d, h).wait_recv()
+            for p in range(prompts):
+                st[h, p * DK : (p + 1) * DK, :] = sin[h * prompts + p].astype(f32)
+
+        @pl.loop(0, pairs)
+        def _(pair):
+            rows = pl.ds(pl.multiple_of(pair * 2 * n, 2 * n), 2 * n)
+            for h in members:
+                hk, hv = slice(h * DK, (h + 1) * DK), slice(h * DV, (h + 1) * DV)
+                state = st[h]
+                from_state = dot(each_prompt(sq[rows, hk], prompts), state.astype(bf16))
+                oi[rows, hv] = head_norm(oi[rows, hv].astype(f32) + from_state, h)
+                added = dot(turned(ek[rows, hk], prompts), vs[rows, hv])
+                decay = jnp.transpose(jnp.exp(tots[2 * pair, :, hk] + tots[2 * pair + 1, :, hk]))
+                for p in range(prompts):
+                    at = slice(p * DK, (p + 1) * DK)
+                    st[h, at, :] = state[at] * decay[:, p : p + 1] + added[at]
+            side = pair // (pairs // 2)
+            j = pair - side * (pairs // 2)
+
+            @pl.when(side == me)
+            def _():
+                keep_copy(j, i).start()
+
+            @pl.when(side != me)
+            def _():
+                give_copy(j, i).start()
+
     for i in range(groups):
-        for d in range(1, kv):
-            incoming_copy(d, i).wait_recv()
-    for h in range(heads):
-        for p in range(prompts):
-            st[h, p * DK : (p + 1) * DK, :] = sin[h * prompts + p].astype(f32)
-
-    @pl.loop(0, blocks)
-    def _(block):
-        rows = pl.ds(pl.multiple_of(block * n, n), n)
-        for h in range(heads):
-            hk, hv = slice(h * DK, (h + 1) * DK), slice(h * DV, (h + 1) * DV)
-            state = st[h]
-            from_state = dot(each_prompt(sq[rows, hk], prompts), state.astype(bf16))
-            oi[rows, hv] = head_norm(oi[rows, hv].astype(f32) + from_state, h)
-            added = dot(turned(ek[rows, hk], prompts), vs[rows, hv])
-            decay = jnp.transpose(jnp.exp(tots[block, :, hk]))
-            for p in range(prompts):
-                at = slice(p * DK, (p + 1) * DK)
-                st[h, at, :] = state[at] * decay[:, p : p + 1] + added[at]
-        side = block // (blocks // 2)
-        j = block - side * (blocks // 2)
-
-        @pl.when(side == me)
-        def _():
-            keep_copy(j).start()
-
-        @pl.when(side != me)
-        def _():
-            give_copy(j).start()
+        scan(i)
 
     for d in range(1, kv):
         for h in range(heads):
             local_copy(d, h).wait_send()
+            incoming_copy(d, h).wait_send()
         for i in range(groups):
             total_copy(d, i).wait_send()
-            incoming_copy(d, i).wait_send()
     dec_keep.wait()
     dec_give.wait()
 
-    @pl.loop(0, blocks // 2)
-    def _(j):
-        keep_copy(j).wait()
-        give_copy(j).wait_send()
-        give_copy(j).wait_recv()
+    for i in range(groups):
+        @pl.loop(0, pairs // 2)
+        def _(j):
+            keep_copy(j, i).wait()
+            give_copy(j, i).wait_send()
+            give_copy(j, i).wait_recv()
 
 
 def last_kernel(
@@ -469,7 +522,7 @@
     n_sem, w_sem, s_sem, y_sem, o_sem, a_sem,
 ):
     own = own_pos * prompts
-    chunk = min(256, own)
+    chunk = min(512, own)
     count = own // chunk
     pos = chunk // prompts
     width = w.shape[1]
@@ -590,23 +643,25 @@
             jax.ShapeDtypeStruct((2, DK, heads * 2 * PAD), f32),
             jax.ShapeDtypeStruct((2 * PAD, vw), f32),
         ),
-        in_specs=[ANY, VMEM, ANY, ANY, ANY, ANY, VMEM, VMEM, VMEM, VMEM, VMEM, VMEM, ANY],
+        in_specs=[ANY, VMEM, ANY, ANY, ANY, ANY, VMEM, VMEM, VMEM, ANY, ANY, ANY, ANY],
         out_specs=(ANY, ANY, VMEM, VMEM, VMEM),
         scratch_shapes=[
             pltpu.VMEM(pieces.shape, bf16),
             pltpu.VMEM((rows, width), bf16),
             pltpu.VMEM((2 * PAD, width), bf16),
             pltpu.VMEM((width, qk), bf16),
-            pltpu.VMEM((width, qk), bf16),
+            pltpu.VMEM((width, 2 * qk), bf16),
             pltpu.VMEM((width, vw), bf16),
-            pltpu.VMEM((width, qk), bf16),
+            pltpu.VMEM(mk.shape, bf16),
+            pltpu.VMEM(mq.shape, bf16),
+            pltpu.VMEM(prompt_state.shape, f32),
             pltpu.VMEM((rows, qk), bf16),
             pltpu.VMEM((rows, qk), bf16),
             pltpu.VMEM((rows, vw), bf16),
             pltpu.VMEM((rows, qk), f32),
             pltpu.VMEM((rows, qk), bf16),
             pltpu.VMEM((rows, qk), bf16),
-            pltpu.VMEM((rows, group * DK), bf16),
+            pltpu.VMEM((own, qk), bf16),
             pltpu.VMEM((rows, vw), bf16),
             pltpu.VMEM((blocks, 8, qk), f32),
             pltpu.VMEM((8, qk), f32),
@@ -621,9 +676,10 @@
             pltpu.VMEM((2, seqs, DK, DV), f32),
             pltpu.VMEM((heads, DK, 2 * PAD), f32),
             pltpu.VMEM((2 * PAD, vw), f32),
+            pltpu.VMEM((2 * PAD, vw), f32),
             pltpu.VMEM((2 * PAD, vw), bf16),
             dma((count,)),
-            dma((3 * groups + 1,)),
+            dma((3 * groups + 4,)),
             dma((count,)),
             dma((count,)),
             dma,
@@ -632,12 +688,12 @@
             dma((kv, heads)),
             dma((kv, groups)),
             dma((kv, groups)),
-            dma((kv, groups)),
-            dma((kv, groups)),
+            dma((kv, heads)),
+            dma((kv, heads)),
             dma((heads,)),
-            dma((blocks // 2,)),
-            dma((blocks // 2,)),
-            dma((blocks // 2,)),
+            dma((groups, blocks // 4)),
+            dma((groups, blocks // 4)),
+            dma((groups, blocks // 4)),
             dma,
             dma,
             dma,
@@ -667,7 +723,7 @@
             pltpu.VMEM(cols.shape, f32),
             pltpu.VMEM(v_rows.shape, f32),
             pltpu.VMEM(prompt_state.shape, f32),
-            dma((count,)),
+            dma((own // min(512, own),)),
             dma((heads,)),
             dma((heads,)),
             dma((heads,)),

time: 85 us -> 81.4 us (0.958)
  Pallas kernels: 84 us -> 80.3 us
    pallas_call x1, Pallas kernels: 68.1 us -> 65.2 us  [on_device(): pl.pallas_call(functools.partial(main_kernel, own_pos, prompts, heads, kv...]
    pallas_call x1, Pallas kernels: 15.9 us -> 15.1 us  [on_device(): pl.pallas_call(functools.partial(last_kernel, own_pos, prompts, heads, de...]
where the time goes in v3:
time: 81.4 us; the launch traced here: 81.1 us
  Pallas kernels  80.3 us (99%)
    pallas_call x1, Pallas kernels, on_device(): pl.pallas_call(functools.partial(main_kernel, own_pos, prompts, heads, kv...  65.2 us
    pallas_call x1, Pallas kernels, on_device(): pl.pallas_call(functools.partial(last_kernel, own_pos, prompts, heads, de...  15.1 us

profile of v3, /device:TPU:0, one launch (start us, length us, event | category | flops | bytes accessed | tf_op | source)
XLA Modules:
  0.0 81.1 jit_solution(18403505352259324036)
XLA Ops:
  0.6 65.2 %layer.1 = (bf16[1024,2048]{1,0:T(8,128)(2,1)}, bf16[16,2048]{1,0:T(8,128)(2,1)}, f32[2,4,32,256]{3,2,1,0:T(8,128)}, f32[2,128,128]{2,1,0:T(8,128)}, f32[32,1024]{1,0:T(8,128)}) custom-call(bf16[512,2,2048]{2,1,0:T(2,128)(2,1)} %x_hbm.1, bf16[8,2048]{1,0:T(8,128)(2,1)} %dec_ref.1, bf16[2048,512]{1,0:T(8,128)(2,1)} %wq_hbm.1, bf16[2048,512]{1,0:T(8,128)(2,1)} %wk_hbm.1, ...), custom_call_target="tpu_custom_call" | custom-call | tf_op jit(solution)/shard_map/layer/pallas_call | solution.py:636
  65.9 15.1 %last.1 = (bf16[512,2,2048]{2,1,0:T(2,128)(2,1)}, bf16[8,2048]{1,0:T(8,128)(2,1)}, f32[2,4,32,256]{3,2,1,0:T(8,128)}, f32[16,4,128,256]{3,2,1,0:T(8,128)}) custom-call(bf16[1024,2048]{1,0:T(8,128)(2,1)} %get-tuple-element.9.nrm_hbm, bf16[16,2048]{1,0:T(8,128)(2,1)} %get-tuple-element.10.ndec_hbm, bf16[2048,2048]{1,0:T(8,128)(2,1)} %w_hbm.1, ...), custom_call_target="tpu_custom_call" | custom-call | tf_op jit(solution)/shard_map/last/pallas_call | solution.py:706
